TPU v7x, 32 devices: a whole 2x2x4 slice. The times are simulated.
32 devices in a mesh: sp: 4 (over z), fs: 4 (over y, x), tp: 2 (over core).
Axes of the slice: x: 2, y: 2, z: 4, core: 2. Of those that a mesh axis runs over, the one named last changes fastest.
Arguments:
- inputs: bfloat16 [4, 512, 2048], P('fs', 'sp'), may hold values from -6 to 6
- input_norm_gain: bfloat16 [2048], replicated, may hold values from 0.099609375 to 1.8984375
- receptance_matrix: bfloat16 [2048, 1024], P('fs', 'tp'), may hold values from -0.125 to 0.125
- key_matrix: bfloat16 [2048, 1024], P('fs', 'tp'), may hold values from -0.125 to 0.125
- value_matrix: bfloat16 [2048, 1024], P('fs', 'tp'), may hold values from -0.125 to 0.125
- pooling_input_weight: bfloat16 [2048, 1024], P('fs', 'tp'), may hold values from -0.125 to 0.125
- decay_lower_matrix: bfloat16 [2048, 128], replicated, may hold values from -0.125 to 0.125
- decay_raise_matrix: bfloat16 [2, 64, 1024], P(None, None, 'tp'), may hold values from -1 to 1
- decay_offset_bias: float32 [2, 1024], P(None, 'tp'), may hold values from -13 to -3
- removal_lower_matrix: bfloat16 [2048, 128], replicated, may hold values from -0.125 to 0.125
- removal_raise_matrix: bfloat16 [2, 64, 1024], P(None, None, 'tp'), may hold values from -1 to 1
- removal_rate_bias: float32 [2, 1024], P(None, 'tp'), may hold values from -9 to 1.5
- tempo_scale: float32 [4, 2, 16, 512], P('fs', None, 'tp', 'sp'), may hold values from 0.3 to 3.2, as said below
- sudden_decay_extra: float32 [4, 2, 16, 512], P('fs', None, 'tp', 'sp'), may hold values from -2.8 to 0
- head_norm_gain: bfloat16 [1024], P('tp'), may hold values from 0.099609375 to 1.8984375
- group_mixing_weight: bfloat16 [4, 256, 256], P('tp'), may hold values from -0.375 to 0.375
- attention_output_matrix: bfloat16 [2048, 1024], P('fs', 'tp'), may hold values from -0.125 to 0.125
- pooling_output_matrix: bfloat16 [2048, 1024], P('fs', 'tp'), may hold values from -0.125 to 0.125
Outputs:
- mixed_out: bfloat16 [4, 512, 2048], P('fs', ('sp', 'tp'))
Inputs may be any that keep to these rules, and one draw needn't show every extreme that they name: `tempo_scale`: positive.
All inputs are finite; a program needn't handle non-finite values.
Results may differ from a plain program's by a relative error of at most 0.017.
Values may be sent and summed in bfloat16 or wider, within the bound.
A program may use at most 128 MiB of HBM per device.

v0:
```python
import functools

import jax
import jax.numpy as jnp
from jax import lax
from jax.experimental import pallas as pl
from jax.experimental.pallas import tpu as pltpu
from jax.sharding import PartitionSpec as P

HEAD = 64
GROUP_WIDTH = 256
LANES = 128
BLOCK = 16
HALO = 16

norm_eps = 1e-06
head_eps = 0.00064
unit_eps = 1e-06
f32 = jnp.float32
bf16 = jnp.bfloat16
VMEM = pl.BlockSpec(memory_space=pltpu.VMEM)


def dot(left, right):
    return jnp.dot(left.astype(bf16), right.astype(bf16), preferred_element_type=f32)


def dot_general(left, right, dims):
    return lax.dot_general(
        left.astype(bf16), right.astype(bf16), (dims, ((), ())), preferred_element_type=f32
    )


def dot_rows(left, right):
    return dot_general(left, right, ((1,), (1,)))


def dot_cols(left, right):
    return dot_general(left, right, ((0,), (0,)))


def exact_dot(left, right, dims):
    return lax.dot_general(
        left, right, (dims, ((), ())), preferred_element_type=f32, precision=lax.Precision.HIGHEST
    )


def remote(src, dst, send, recv, axis, peer):
    return pltpu.make_async_remote_copy(
        src_ref=src,
        dst_ref=dst,
        send_sem=send,
        recv_sem=recv,
        device_id={axis: peer},
        device_id_type=pl.DeviceIdType.MESH,
    )


def greet(barrier, axis, peer):
    pl.semaphore_signal(
        barrier, inc=1, device_id={axis: peer}, device_id_type=pl.DeviceIdType.MESH
    )


def flipped(at, bits):
    moved = at
    bit = 1
    while bit <= bits:
        if bits & bit:
            moved = moved + bit - 2 * bit * lax.rem(at // bit, 2)
        bit *= 2
    return moved


def front_part(
    n,
    x_ref,
    gain_ref,
    weights,
    lowers,
    loads,
    pool_ref,
    lat_ref,
    mine,
    cells,
    part,
    pool_part,
    landed,
    pool_landed,
    xs,
    xr,
    ps,
    pr,
    count,
    mix_pair,
):
    me = lax.axis_index("fs")
    core, ntp = lax.axis_index("tp"), lax.axis_size("tp")
    width = x_ref.shape[2] // n
    share = x_ref.shape[1] // ntp
    rows = pl.ds(pl.multiple_of(core * share, share), share)
    pairs = part.shape[1]
    x = x_ref[0].astype(f32)
    normed = (
        x
        * lax.rsqrt(jnp.mean(x * x, axis=-1, keepdims=True) + norm_eps)
        * gain_ref[...].astype(f32).reshape(1, -1)
    ).astype(bf16)
    for j in range(n):
        mine[j] = normed[:, j * width : (j + 1) * width]
    pl.semaphore_wait(pltpu.get_barrier_semaphore(), count)
    order = list(range(n - 1, 0, -1))
    moves = []
    for d in order:
        peer = flipped(me, d)
        copy = remote(
            mine.at[peer, rows], cells.at[me, rows], xs.at[d, 0], xr.at[d, 0], "fs", peer
        )
        copy.start()
        moves.append(copy)
    for load in loads[:2]:
        load.wait()
    dl_ref, rl_ref = lowers
    decay = jnp.zeros((x.shape[0], dl_ref.shape[1]), f32)
    rate = jnp.zeros((x.shape[0], rl_ref.shape[1]), f32)
    for j in range(n):
        block = mine[j]
        decay = decay + dot(block, dl_ref[j * width : (j + 1) * width])
        rate = rate + dot(block, rl_ref[j * width : (j + 1) * width])
    lat_ref[0] = jnp.tanh(decay.astype(bf16).astype(f32)).astype(bf16)
    lat_ref[1] = rate.astype(bf16)
    for load in loads[2:]:
        load.wait()
    for d, copy in zip(order, list(moves)):
        peer = flipped(me, d)
        copy.wait_recv()
        for e in range(1, ntp):
            passed = remote(
                cells.at[peer, rows],
                cells.at[peer, rows],
                xs.at[d, e],
                xr.at[d, e],
                "tp",
                lax.rem(core + e, ntp),
            )
            passed.start()
            moves.append(passed)
    for copy in moves[len(order) :]:
        copy.wait_recv()

    def pair_copy(d, p):
        peer = flipped(me, d)
        return remote(
            part.at[peer, p], landed.at[me, p], ps.at[d, p], pr.at[d, p], "fs", peer
        )

    def pool_copy(d):
        peer = flipped(me, d)
        return remote(
            pool_part.at[peer],
            pool_landed.at[me],
            ps.at[d, pairs],
            pr.at[d, pairs],
            "fs",
            peer,
        )

    for p in range(pairs):
        for d in order:
            peer = flipped(me, d)
            for m in range(3):
                part[peer, p, m] = dot(
                    cells[peer], weights[m][:, p * LANES : (p + 1) * LANES]
                ).astype(bf16)
            pair_copy(d, p).start()
    for d in order:
        peer = flipped(me, d)
        pool_part[peer] = dot(cells[peer], weights[3][...]).astype(bf16)
        pool_copy(d).start()

    def pair_step(p, carry):
        lanes = pl.ds(pl.multiple_of(p * LANES, LANES), LANES)
        owned = [dot(mine[me], weights[m][:, lanes]) for m in range(3)]
        for d in range(1, n):
            pair_copy(d, p).wait_recv()
        for d in range(1, n):
            peer = flipped(me, d)
            owned = [o + landed[peer, p, m].astype(f32) for m, o in enumerate(owned)]
        mix_pair(p, lanes, *[o.astype(bf16) for o in owned])
        return carry

    lax.fori_loop(0, pairs, pair_step, 0)
    total = dot(mine[me], weights[3][...])
    for d in range(1, n):
        pool_copy(d).wait_recv()
    for d in range(1, n):
        total = total + pool_landed[flipped(me, d)].astype(f32)
    pool_ref[...] = total.astype(bf16)
    for copy in moves:
        copy.wait_send()
    for d in range(1, n):
        for p in range(pairs):
            pair_copy(d, p).wait_send()
        pool_copy(d).wait_send()


def mix_pair(
    pair,
    lanes,
    key,
    receptance,
    value,
    lat_ref,
    draise_ref,
    dbias_ref,
    rraise_ref,
    rbias_ref,
    tempo_ref,
    extra_ref,
    query_ref,
    local_ref,
    transfer_ref,
    carried_ref,
):
    tokens = key.shape[0]
    kf = key.astype(f32)
    rf = receptance.astype(f32)
    lane = lax.broadcasted_iota(jnp.int32, (tokens, LANES), 1)
    row = lax.broadcasted_iota(jnp.int32, (tokens, LANES), 0)
    head0 = lane < HEAD
    k2 = kf * kf
    s0 = jnp.sum(jnp.where(head0, k2, 0.0), axis=-1, keepdims=True)
    s1 = jnp.sum(jnp.where(head0, 0.0, k2), axis=-1, keepdims=True)
    unit = kf * lax.rsqrt(jnp.where(head0, s0, s1) + unit_eps)
    heads = tempo_ref.shape[1]
    spread = (
        lax.broadcasted_iota(jnp.int32, (heads, LANES), 0)
        == 2 * pair + lax.broadcasted_iota(jnp.int32, (heads, LANES), 1) // HEAD
    ).astype(f32)
    blocks = tokens // BLOCK
    zero_row = jnp.zeros((1, LANES), f32)
    eye = (row == lane).astype(f32)
    sizes = []
    size = 1
    while size < tokens:
        sizes.append(size)
        size *= 2

    def level_mask(k):
        return ((row >> (k + 1)) == (lane >> (k + 1))) & ((row >> k) != (lane >> k))

    ways = []
    for d in range(2):
        lat_mask = head0 if d == 0 else ~head0
        lat_d = jnp.where(lat_mask, lat_ref[0].astype(f32), 0.0)
        lat_r = jnp.where(lat_mask, lat_ref[1].astype(f32), 0.0)
        pre = dbias_ref[d : d + 1, lanes] + dot(lat_d, draise_ref[:, lanes])
        velocity = jax.nn.sigmoid(pre) * 0.6065306597126334
        tempo = exact_dot(tempo_ref[d], spread, ((0,), (0,)))
        extra = exact_dot(extra_ref[d], spread, ((0,), (0,)))
        ld = -velocity * tempo + extra
        rate = jax.nn.sigmoid(rbias_ref[d : d + 1, lanes] + dot(lat_r, rraise_ref[:, lanes]))
        removal = unit * rate
        written = kf * rate
        upto = (lane <= row) if d == 0 else (lane >= row)
        inner = exact_dot(upto.astype(f32), ld, ((1,), (0,)))
        excl = inner - ld
        grams = []
        for i in range(blocks):
            lo, hi = i * BLOCK, (i + 1) * BLOCK
            if d == 0:
                base = inner[lo - 1 : lo] if i > 0 else zero_row
            else:
                base = inner[hi : hi + 1] if i < blocks - 1 else zero_row
            ahead = unit[lo:hi] * jnp.exp(excl[lo:hi] - base)
            query = rf[lo:hi] * jnp.exp(inner[lo:hi] - base)
            grow = jnp.exp(jnp.minimum(base - inner, 80.0))
            right = jnp.concatenate([(removal * grow).astype(bf16), (written * grow).astype(bf16)], 0)
            h0 = head0[lo:hi]
            left = jnp.concatenate(
                [
                    jnp.where(h0, ahead, 0.0),
                    jnp.where(h0, 0.0, ahead),
                    jnp.where(h0, query, 0.0),
                    jnp.where(h0, 0.0, query),
                ],
                0,
            )
            grams.append(dot_rows(left, right))
        strict = (lane < row) if d == 0 else (lane > row)

        def gathered(place, at, mask):
            rows = jnp.concatenate(
                [g[place * BLOCK : (place + 1) * BLOCK, at * tokens : (at + 1) * tokens] for g in grams],
                0,
            )
            return jnp.where(mask, rows, 0.0)

        way = dict(inner=inner, excl=excl, removal=removal, written=written)
        way["link"] = [gathered(h, 0, strict) for h in range(2)]
        way["link_write"] = [gathered(h, 1, strict).astype(bf16) for h in range(2)]
        way["read"] = [gathered(2 + h, 0, upto).astype(bf16) for h in range(2)]
        way["read_write"] = [gathered(2 + h, 1, upto).astype(bf16) for h in range(2)]
        ways.append(way)

    links = [way["link"][h] for way in ways for h in range(2)]
    inverses = [eye - jnp.where(level_mask(0), a, 0.0) for a in links]
    for k in range(1, len(sizes)):
        mask = level_mask(k)
        firsts = [dot(t, jnp.where(mask, a, 0.0)) for t, a in zip(inverses, links)]
        inverses = [t - dot(u, t) for t, u in zip(inverses, firsts)]

    block_diag = (row < HEAD) == head0
    local = jnp.zeros((tokens, LANES), f32)
    for d, way in enumerate(ways):
        inner, excl = way["inner"], way["excl"]
        last = inner[tokens - 1 : tokens] if d == 0 else inner[0:1]
        ahead = unit * jnp.exp(excl)
        query = rf * jnp.exp(inner)
        tail = jnp.exp(last - inner)

        def chosen(pieces):
            return jnp.where(head0, pieces[0], pieces[1])

        base = chosen([dot(way["link_write"][h], value) for h in range(2)])
        rhs = jnp.concatenate([ahead.astype(bf16), base.astype(bf16)], 1)
        solved = [dot(inverses[2 * d + h], rhs) for h in range(2)]
        pull_map = -chosen([s[:, :LANES] for s in solved])
        pull_base = -chosen([s[:, LANES:] for s in solved])
        remove_tail = (way["removal"] * tail).astype(bf16)
        write_tail = (way["written"] * tail).astype(bf16)
        both = jnp.concatenate([pull_map.astype(bf16), pull_base.astype(bf16)], 1)
        seen = [dot(way["read"][h], both) for h in range(2)]
        query_ref[d, :, lanes] = (query + chosen([s[:, :LANES] for s in seen])).astype(bf16)
        local = (
            local
            + chosen([s[:, LANES:] for s in seen])
            + chosen([dot(way["read_write"][h], value) for h in range(2)])
        )
        transfer = jnp.where(block_diag, dot_cols(pull_map, remove_tail), 0.0) + eye * jnp.exp(last)
        transfer_ref[d, pair] = transfer
        carried = dot_cols(
            jnp.concatenate([pull_base.astype(bf16), value], 0),
            jnp.concatenate([remove_tail, write_tail], 0),
        )
        carried = jnp.where(block_diag, carried, 0.0)
        carried_ref[d, pair] = carried[:HEAD] + carried[HEAD:]
    local_ref[:, lanes] = local


def layer_kernel(
    nsp,
    nfs,
    ntp,
    x_ref,
    in_gain_ref,
    wk_hbm,
    wr_hbm,
    wv_hbm,
    wi_hbm,
    dl_hbm,
    rl_hbm,
    draise_ref,
    dbias_ref,
    rraise_ref,
    rbias_ref,
    tempo_ref,
    extra_ref,
    mix_hbm,
    gain_ref,
    wa_hbm,
    wp_hbm,
    out_ref,
    wk_ref,
    wr_ref,
    wv_ref,
    wi_ref,
    dl_ref,
    rl_ref,
    mix_ref,
    wa_ref,
    wp_ref,
    loaded,
    mine,
    cells,
    part,
    pool_part,
    landed,
    pool_landed,
    xs,
    xr,
    ps,
    pr,
    lat_ref,
    pool_ref,
    query_ref,
    local_ref,
    transfer_ref,
    carried_ref,
    edge,
    halo,
    incoming,
    leaving,
    act,
    tsend,
    trecv,
    osend,
    orecv,
    hs,
    hr,
    ss,
    sr,
    gs,
    gr,
    ts,
    tr,
    os,
    orr,
):
    z = lax.axis_index("sp")
    me = lax.axis_index("fs")
    core = lax.axis_index("tp")
    tokens, channels = local_ref.shape
    pairs = transfer_ref.shape[1]
    half_rows = tokens // ntp
    has_prev = z > 0
    has_next = z < nsp - 1
    prev = jnp.maximum(z - 1, 0)
    after = jnp.minimum(z + 1, nsp - 1)

    barrier = pltpu.get_barrier_semaphore()
    for d in range(1, nfs):
        greet(barrier, "fs", flipped(me, d))
    for d in range(1, ntp):
        greet(barrier, "tp", lax.rem(core + d, ntp))
    pl.when(has_prev)(lambda: greet(barrier, "sp", prev))
    pl.when(has_next)(lambda: greet(barrier, "sp", after))
    count = nfs + ntp - 2 + jnp.where(has_prev, 1, 0) + jnp.where(has_next, 1, 0)
    sources = (dl_hbm, rl_hbm, wk_hbm, wr_hbm, wv_hbm, wi_hbm, mix_hbm, wa_hbm, wp_hbm)
    targets = (dl_ref, rl_ref, wk_ref, wr_ref, wv_ref, wi_ref, mix_ref, wa_ref, wp_ref)
    loads = [
        pltpu.make_async_copy(source, target, loaded.at[i])
        for i, (source, target) in enumerate(zip(sources, targets))
    ]
    for load in loads:
        load.start()
    front_part(
        nfs,
        x_ref,
        in_gain_ref,
        (wk_ref, wr_ref, wv_ref, wi_ref),
        (dl_ref, rl_ref),
        loads[:6],
        pool_ref,
        lat_ref,
        mine,
        cells,
        part,
        pool_part,
        landed,
        pool_landed,
        xs,
        xr,
        ps,
        pr,
        count,
        lambda pair, lanes, key, receptance, value: mix_pair(
            pair,
            lanes,
            key,
            receptance,
            value,
            lat_ref,
            draise_ref,
            dbias_ref,
            rraise_ref,
            rbias_ref,
            tempo_ref,
            extra_ref,
            query_ref,
            local_ref,
            transfer_ref,
            carried_ref,
        ),
    )
    for load in loads[6:]:
        load.wait()
    edge[0] = pool_ref[:HALO]
    edge[1] = pool_ref[tokens - HALO :]

    sides = [(has_prev, prev, has_next), (has_next, after, has_prev)]
    def state_copy(d, p):
        return remote(
            leaving.at[d, p],
            incoming.at[d, p],
            ss.at[d, p],
            sr.at[d, p],
            "sp",
            after if d == 0 else prev,
        )

    halo_copies = [
        remote(edge.at[1], halo.at[0], hs.at[0], hr.at[0], "sp", after),
        remote(edge.at[0], halo.at[1], hs.at[1], hr.at[1], "sp", prev),
    ]
    sends = [has_next, has_prev]
    takes = [has_prev, has_next]

    def relay(d):
        @pl.when(jnp.logical_not(takes[d]))
        def _():
            incoming[d] = jnp.zeros_like(incoming[d])

        for p in range(pairs):

            @pl.when(takes[d])
            def _():
                state_copy(d, p).wait_recv()

            @pl.when(sends[d])
            def _():
                leaving[d, p] = (
                    dot(incoming[d, p], transfer_ref[d, p]) + carried_ref[d, p]
                ).astype(bf16)
                state_copy(d, p).start()

    def start_halo(d):
        pl.when(sends[d])(lambda: halo_copies[d].start())

    early = 2 * z < nsp

    @pl.when(early)
    def _():
        relay(0)

    @pl.when(jnp.logical_not(early))
    def _():
        relay(1)

    for d in range(2):
        start_halo(d)
    for d in range(2):

        @pl.when(takes[d])
        def _():
            halo_copies[d].wait_recv()

        @pl.when(jnp.logical_not(takes[d]))
        def _():
            halo[d] = jnp.zeros_like(halo[d])

    span = tokens + 2 * HALO
    rim = jnp.concatenate([halo[0], pool_ref[...], halo[1]], 0)
    here = lax.broadcasted_iota(jnp.int32, (tokens, span), 0)
    there = lax.broadcasted_iota(jnp.int32, (tokens, span), 1) - HALO
    position = z * tokens + lax.broadcasted_iota(jnp.int32, (tokens, GROUP_WIDTH), 0)
    length = tokens * nsp
    groups_here = channels // GROUP_WIDTH
    for member in range(groups_here):
        cols = slice(member * GROUP_WIDTH, (member + 1) * GROUP_WIDTH)
        reach = jnp.left_shift(1, core * groups_here + member)
        window = jnp.where((there >= here - reach) & (there < here + reach), 1.0, 0.0)
        total = dot(window, rim[:, cols])
        size = (
            jnp.minimum(position + reach, length) - jnp.maximum(position - reach, 0)
        ).astype(f32)
        diff = (total / size - pool_ref[:, cols].astype(f32)).astype(bf16)
        act[me, 0, :, cols] = dot(diff, mix_ref[member]).astype(bf16)
    order = list(range(nfs - 1, 0, -1))
    shares = []
    for d in order:
        peer = flipped(me, d)
        copy = remote(act.at[me, 0], act.at[me, 0], gs.at[d, 0], gr.at[d, 0], "fs", peer)
        copy.start()
        shares.append(copy)

    @pl.when(early)
    def _():
        relay(1)

    @pl.when(jnp.logical_not(early))
    def _():
        relay(0)

    head0 = lax.broadcasted_iota(jnp.int32, (tokens, LANES), 1) < HEAD
    top0 = lax.broadcasted_iota(jnp.int32, (HEAD, LANES), 1) < HEAD
    for p in range(pairs):
        lanes = slice(p * LANES, (p + 1) * LANES)
        readout = local_ref[:, lanes]
        for d in range(2):
            state = incoming[d, p].astype(f32)
            wide = jnp.concatenate(
                [jnp.where(top0, state, 0.0), jnp.where(top0, 0.0, state)], 0
            )
            readout = readout + dot_rows(query_ref[d, :, lanes], wide)

        def head_mean(cells):
            low = jnp.sum(jnp.where(head0, cells, 0.0), axis=-1, keepdims=True)
            high = jnp.sum(jnp.where(head0, 0.0, cells), axis=-1, keepdims=True)
            return jnp.where(head0, low, high) * (1.0 / HEAD)

        centred = readout - head_mean(readout)
        scaled = centred * lax.rsqrt(head_mean(centred * centred) + head_eps)
        act[me, 1, :, lanes] = (scaled * gain_ref[lanes].astype(f32).reshape(1, -1)).astype(bf16)
        if (p + 1) % (pairs // 2) == 0:
            part = (p + 1) // (pairs // 2)
            cols = pl.ds((part - 1) * (channels // 2), channels // 2)
            for d in order:
                copy = remote(
                    act.at[me, 1, :, cols],
                    act.at[me, 1, :, cols],
                    gs.at[d, part],
                    gr.at[d, part],
                    "fs",
                    flipped(me, d),
                )
                copy.start()
                shares.append(copy)

    other = lax.rem(core + 1, ntp)
    mine_at = pl.multiple_of(core * half_rows, half_rows)
    other_at = pl.multiple_of(other * half_rows, half_rows)

    def product(seq, rows):
        return dot_rows(act[seq, 1, rows], wa_ref[...]) + dot_rows(act[seq, 0, rows], wp_ref[...])

    returns = []
    swaps = []
    turns = [0] + order
    for d in turns:
        seq = flipped(me, d)
        if d:
            for copy, at in zip(shares, order * 3):
                if at == d:
                    copy.wait_recv()
        tsend[d] = product(seq, pl.ds(other_at, half_rows)).astype(bf16)
        swap = remote(tsend.at[d], trecv.at[d], ts.at[d], tr.at[d], "tp", other)
        swap.start()
        swaps.append(swap)
        kept = product(seq, pl.ds(mine_at, half_rows))
        swap.wait_recv()
        whole = (kept + trecv[d].astype(f32)).astype(bf16)
        if d:
            osend[d] = whole
            copy = remote(osend.at[d], orecv.at[me], os.at[d], orr.at[d], "fs", seq)
            copy.start()
            returns.append(copy)
        else:
            orecv[me] = whole
    for copy in returns:
        copy.wait_recv()
    for j in range(nfs):
        out_ref[0, :, j * channels : (j + 1) * channels] = orecv[j]
    for copy in shares + swaps + returns:
        copy.wait_send()
    for d in range(2):

        @pl.when(sends[d])
        def _():
            for p in range(pairs):
                state_copy(d, p).wait_send()
            halo_copies[d].wait_send()


def shards(
    inputs,
    input_norm_gain,
    receptance_matrix,
    key_matrix,
    value_matrix,
    pooling_input_weight,
    decay_lower_matrix,
    decay_raise_matrix,
    decay_offset_bias,
    removal_lower_matrix,
    removal_raise_matrix,
    removal_rate_bias,
    tempo_scale,
    sudden_decay_extra,
    head_norm_gain,
    group_mixing_weight,
    attention_output_matrix,
    pooling_output_matrix,
):
    nsp, nfs, ntp = lax.axis_size("sp"), lax.axis_size("fs"), lax.axis_size("tp")
    _, tokens, features = inputs.shape
    depth, channels = key_matrix.shape
    pairs = channels // LANES
    dma = pltpu.SemaphoreType.DMA
    rank = decay_lower_matrix.shape[1]
    rank2 = decay_raise_matrix.shape[0] * decay_raise_matrix.shape[1]
    anywhere = pl.BlockSpec(memory_space=pl.ANY)
    half = (nfs, tokens // ntp, depth)
    return pl.pallas_call(
        functools.partial(layer_kernel, nsp, nfs, ntp),
        out_shape=jax.ShapeDtypeStruct((1, tokens // ntp, features), bf16),
        in_specs=[VMEM] * 2
        + [anywhere] * 6
        + [VMEM] * 6
        + [anywhere, VMEM, anywhere, anywhere],
        out_specs=VMEM,
        scratch_shapes=[pltpu.VMEM((depth, channels), bf16)] * 4
        + [
            pltpu.VMEM((features, rank), bf16),
            pltpu.VMEM((features, rank), bf16),
            pltpu.VMEM(group_mixing_weight.shape, bf16),
            pltpu.VMEM(attention_output_matrix.shape, bf16),
            pltpu.VMEM(pooling_output_matrix.shape, bf16),
            dma((9,)),
            pltpu.VMEM((nfs, tokens, depth), bf16),
            pltpu.VMEM((nfs, tokens, depth), bf16),
            pltpu.VMEM((nfs, pairs, 3, tokens, LANES), bf16),
            pltpu.VMEM((nfs, tokens, channels), bf16),
            pltpu.VMEM((nfs, pairs, 3, tokens, LANES), bf16),
            pltpu.VMEM((nfs, tokens, channels), bf16),
            dma((nfs, ntp)),
            dma((nfs, ntp)),
            dma((nfs, pairs + 1)),
            dma((nfs, pairs + 1)),
            pltpu.VMEM((2, tokens, rank), bf16),
            pltpu.VMEM((tokens, channels), bf16),
            pltpu.VMEM((2, tokens, channels), bf16),
            pltpu.VMEM((tokens, channels), f32),
            pltpu.VMEM((2, pairs, LANES, LANES), f32),
            pltpu.VMEM((2, pairs, HEAD, LANES), f32),
            pltpu.VMEM((2, HALO, channels), bf16),
            pltpu.VMEM((2, HALO, channels), bf16),
            pltpu.VMEM((2, pairs, HEAD, LANES), bf16),
            pltpu.VMEM((2, pairs, HEAD, LANES), bf16),
            pltpu.VMEM((nfs, 2, tokens, channels), bf16),
            pltpu.VMEM(half, bf16),
            pltpu.VMEM(half, bf16),
            pltpu.VMEM(half, bf16),
            pltpu.VMEM(half, bf16),
            dma((2,)),
            dma((2,)),
            dma((2, pairs)),
            dma((2, pairs)),
            dma((nfs, 3)),
            dma((nfs, 3)),
            dma((nfs,)),
            dma((nfs,)),
            dma((nfs,)),
            dma((nfs,)),
        ],
        compiler_params=pltpu.CompilerParams(
            collective_id=0, has_side_effects=True, vmem_limit_bytes=60 * 1024 * 1024
        ),
        name="layer",
    )(
        inputs,
        input_norm_gain,
        key_matrix,
        receptance_matrix,
        value_matrix,
        pooling_input_weight,
        decay_lower_matrix,
        removal_lower_matrix,
        decay_raise_matrix.reshape(rank2, channels),
        decay_offset_bias,
        removal_raise_matrix.reshape(rank2, channels),
        removal_rate_bias,
        tempo_scale[0],
        sudden_decay_extra[0],
        group_mixing_weight,
        head_norm_gain,
        attention_output_matrix,
        pooling_output_matrix,
    )


def solution(mesh):
    in_specs = (
        P("fs", "sp", None),
        P(),
        P("fs", "tp"),
        P("fs", "tp"),
        P("fs", "tp"),
        P("fs", "tp"),
        P(),
        P(None, None, "tp"),
        P(None, "tp"),
        P(),
        P(None, None, "tp"),
        P(None, "tp"),
        P("fs", None, "tp", "sp"),
        P("fs", None, "tp", "sp"),
        P("tp"),
        P("tp", None, None),
        P("fs", "tp"),
        P("fs", "tp"),
    )
    out_specs = P("fs", ("sp", "tp"), None)
    return jax.shard_map(shards, mesh=mesh, in_specs=in_specs, out_specs=out_specs, check_vma=False)
```

profile of v0, /device:TPU:0, one launch (start us, length us, event | category | flops | bytes accessed | tf_op | source)
XLA Modules:
  0.0 64.8 jit_solution(16902383792678042496)
XLA Ops:
  0.0 63.1 %layer.1 = bf16[1,64,2048]{2,1,0:T(8,128)(2,1)} custom-call(bf16[1,128,2048]{2,1,0:T(8,128)(2,1)} %x_ref.1, bf16[2048]{0:T(1024)(128)(2,1)} %in_gain_ref.1, bf16[512,512]{1,0:T(8,128)(2,1)} %wk_hbm.1, bf16[512,512]{1,0:T(8,128)(2,1)} %wr_hbm.1, bf16[512,512]{1,0:T(8,128)(2,1)} %wv_hbm.1, bf16[512,512]{1,0:T(8,128)(2,1)} %wi_hbm.1, bf16[2048,128]{1,0:T(8,128)(2,1)} %dl_hbm.1, ...), custom_call_target="tpu_custom_call" | custom-call | tf_op jit(solution)/shard_map/layer/pallas_call | solution.py:694
  63.1 1.7 %copy.20 = bf16[1,64,2048]{2,1,0:T(8,128)(2,1)} copy(bf16[1,64,2048]{2,1,0:T(8,128)(2,1)} %layer.1) | data formatting | bytes 524288
where the time goes:
time: 64.9 us; the launch traced here: 64.8 us
  Pallas kernels  63.1 us (97%)
  local copies, waits for them, and re-layouts  1.67 us (3%)
    pallas_call x1, Pallas kernels, shards(): pl.pallas_call(functools.partial(layer_kernel, nsp, nfs, ntp), out_shape=...  63.1 us
    unnamed x1, local copies, waits for them, and re-layouts  1.67 us

commit v1 on v0

v1 whole, which is shorter than its diff:
```python
import functools

import jax
import jax.numpy as jnp
from jax import lax
from jax.experimental import pallas as pl
from jax.experimental.pallas import tpu as pltpu
from jax.sharding import PartitionSpec as P

HEAD = 64
GROUP_WIDTH = 256
LANES = 128
BLOCK = 16
HALO = 16
PER = 2

norm_eps = 1e-06
head_eps = 0.00064
unit_eps = 1e-06
f32 = jnp.float32
bf16 = jnp.bfloat16
VMEM = pl.BlockSpec(memory_space=pltpu.VMEM)


def dot(left, right):
    return jnp.dot(left.astype(bf16), right.astype(bf16), preferred_element_type=f32)


def dot_general(left, right, dims):
    return lax.dot_general(
        left.astype(bf16), right.astype(bf16), (dims, ((), ())), preferred_element_type=f32
    )


def dot_rows(left, right):
    return dot_general(left, right, ((1,), (1,)))


def dot_cols(left, right):
    return dot_general(left, right, ((0,), (0,)))


def split_exact(cells, pieces):
    parts = []
    for _ in range(pieces - 1):
        high = cells.astype(bf16).astype(f32)
        parts.append(high)
        cells = cells - high
    return parts + [cells]


def remote(src, dst, send, recv, axis, peer):
    return pltpu.make_async_remote_copy(
        src_ref=src,
        dst_ref=dst,
        send_sem=send,
        recv_sem=recv,
        device_id={axis: peer},
        device_id_type=pl.DeviceIdType.MESH,
    )


def greet(barrier, axis, peer):
    pl.semaphore_signal(
        barrier, inc=1, device_id={axis: peer}, device_id_type=pl.DeviceIdType.MESH
    )


def flipped(at, bits):
    moved = at
    bit = 1
    while bit <= bits:
        if bits & bit:
            moved = moved + bit - 2 * bit * lax.rem(at // bit, 2)
        bit *= 2
    return moved


def front_part(
    n,
    x_ref,
    gain_ref,
    weights,
    lowers,
    loads,
    pool_ref,
    lat_ref,
    mine,
    cells,
    part,
    pool_part,
    onward,
    pool_onward,
    landed,
    pool_landed,
    joined,
    pool_joined,
    xs,
    xr,
    ps,
    pr,
    qs,
    qr,
    count,
    mix_group,
):
    me = lax.axis_index("fs")
    core, ntp = lax.axis_index("tp"), lax.axis_size("tp")
    width = x_ref.shape[2] // n
    share = x_ref.shape[1] // ntp
    rows = pl.ds(pl.multiple_of(core * share, share), share)
    groups = part.shape[0]
    wide = part.shape[4]
    x = x_ref[0].astype(f32)
    with jax.named_scope("norm"):
        normed = (
            x
            * lax.rsqrt(jnp.mean(x * x, axis=-1, keepdims=True) + norm_eps)
            * gain_ref[...].astype(f32).reshape(1, -1)
        ).astype(bf16)
        for j in range(n):
            mine[j] = normed[:, j * width : (j + 1) * width]
    with jax.named_scope("barrier"):
        pl.semaphore_wait(pltpu.get_barrier_semaphore(), count)
    order = list(range(n - 1, 0, -1))
    moves = []
    for d in order:
        peer = flipped(me, d)
        copy = remote(
            mine.at[peer, rows], cells.at[me, rows], xs.at[d, 0], xr.at[d, 0], "fs", peer
        )
        copy.start()
        moves.append(copy)
    with jax.named_scope("latent"):
        for load in loads[:2]:
            load.wait()
        dl_ref, rl_ref = lowers
        decay = jnp.zeros((x.shape[0], dl_ref.shape[1]), f32)
        rate = jnp.zeros((x.shape[0], rl_ref.shape[1]), f32)
        for j in range(n):
            block = mine[j]
            decay = decay + dot(block, dl_ref[j * width : (j + 1) * width])
            rate = rate + dot(block, rl_ref[j * width : (j + 1) * width])
        lat_ref[0] = jnp.tanh(decay.astype(bf16).astype(f32)).astype(bf16)
        lat_ref[1] = rate.astype(bf16)
        for load in loads[2:]:
            load.wait()
    with jax.named_scope("xwait"):
        for d, copy in zip(order, list(moves)):
            peer = flipped(me, d)
            copy.wait_recv()
            for e in range(1, ntp):
                passed = remote(
                    cells.at[peer, rows],
                    cells.at[peer, rows],
                    xs.at[d, e],
                    xr.at[d, e],
                    "tp",
                    lax.rem(core + e, ntp),
                )
                passed.start()
                moves.append(passed)
        for copy in moves[len(order) :]:
            copy.wait_recv()

    first, second, across = routes(me, n, core)
    targets = (first, across)

    def first_copy(g, slot):
        return remote(
            part.at[g, slot], landed.at[g, slot], ps.at[g, slot], pr.at[g, slot], "fs", first
        )

    def first_pool(slot):
        return remote(
            pool_part.at[slot],
            pool_landed.at[slot],
            ps.at[groups, slot],
            pr.at[groups, slot],
            "fs",
            first,
        )

    def second_copy(g):
        return remote(onward.at[g], joined.at[g], qs.at[g], qr.at[g], "fs", second)

    second_pool = remote(
        pool_onward, pool_joined, qs.at[groups], qr.at[groups], "fs", second
    )

    def piece(m, g):
        return weights[m][:, g * wide : (g + 1) * wide]

    with jax.named_scope("partials"):
        for g in range(groups):
            for slot in (1, 0):
                for m in range(3):
                    part[g, slot, m] = dot(cells[targets[slot]], piece(m, g)).astype(bf16)
                first_copy(g, slot).start()
        for slot in (1, 0):
            pool_part[slot] = dot(cells[targets[slot]], weights[3][...]).astype(bf16)
            first_pool(slot).start()

    def forward(g):
        with jax.named_scope(f"fwd{g}"):
            first_copy(g, 1).wait_recv()
            for m in range(3):
                onward[g, m] = (
                    dot(cells[second], piece(m, g)) + landed[g, 1, m].astype(f32)
                ).astype(bf16)
            second_copy(g).start()

    def forward_pool():
        with jax.named_scope("fwdpool"):
            first_pool(1).wait_recv()
            pool_onward[...] = (
                dot(cells[second], weights[3][...]) + pool_landed[1].astype(f32)
            ).astype(bf16)
            second_pool.start()

    def settle(g):
        with jax.named_scope(f"settle{g}"):
            first_copy(g, 0).wait_recv()
            second_copy(g).wait_recv()
        with jax.named_scope(f"mix{g}"):
            owned = [
                (
                    dot(mine[me], piece(m, g))
                    + landed[g, 0, m].astype(f32)
                    + joined[g, m].astype(f32)
                ).astype(bf16)
                for m in range(3)
            ]
            mix_group(g, *owned)

    for g in range(groups):
        forward(g)
    for g in range(groups):
        settle(g)
        if g == 0:
            forward_pool()
    with jax.named_scope("poolin"):
        first_pool(0).wait_recv()
        second_pool.wait_recv()
        pool_ref[...] = (
            dot(mine[me], weights[3][...])
            + pool_landed[0].astype(f32)
            + pool_joined[...].astype(f32)
        ).astype(bf16)

    def finish():
        for copy in moves:
            copy.wait_send()
        for g in range(groups):
            for slot in (1, 0):
                first_copy(g, slot).wait_send()
            second_copy(g).wait_send()
        for slot in (1, 0):
            first_pool(slot).wait_send()
        second_pool.wait_send()

    return finish


def routes(me, n, core):
    low, high = flipped(me, 1), flipped(me, n // 2)
    odd = lax.rem(core, 2)
    return low + odd * (high - low), high + odd * (low - high), flipped(me, n // 2 + 1)


def mix_group(
    g,
    key,
    receptance,
    value,
    lat_ref,
    draise_ref,
    dbias_ref,
    rraise_ref,
    rbias_ref,
    tempo_ref,
    extra_ref,
    query_ref,
    local_ref,
    transfer_ref,
    carried_ref,
):
    tokens, wide = key.shape
    per = wide // LANES
    lanes = slice(g * wide, (g + 1) * wide)
    kf = key.astype(f32)
    rf = receptance.astype(f32)
    lane = lax.broadcasted_iota(jnp.int32, (tokens, LANES), 1)
    row = lax.broadcasted_iota(jnp.int32, (tokens, LANES), 0)
    head0 = lane < HEAD
    only = [head0.astype(f32).astype(bf16), (~head0).astype(f32).astype(bf16)]
    blank = jnp.zeros((tokens, LANES), bf16)

    def cut(cells, j):
        return cells[:, j * LANES : (j + 1) * LANES]

    def both_heads(cells):
        return jnp.concatenate([cells * only[0], cells * only[1]], 0)

    def rows_for_heads(cells):
        return jnp.concatenate(
            [jnp.concatenate([cut(cells, i) * o for i in range(cells.shape[1] // LANES)], 1) for o in only], 0
        )

    units = []
    for j in range(per):
        kj = cut(kf, j)
        k2 = kj * kj
        s0 = jnp.sum(jnp.where(head0, k2, 0.0), axis=-1, keepdims=True)
        s1 = jnp.sum(jnp.where(head0, 0.0, k2), axis=-1, keepdims=True)
        units.append(kj * lax.rsqrt(jnp.where(head0, s0, s1) + unit_eps))
    heads = tempo_ref.shape[1]
    spread = (
        lax.broadcasted_iota(jnp.int32, (heads, wide), 0)
        == 2 * per * g + lax.broadcasted_iota(jnp.int32, (heads, wide), 1) // HEAD
    ).astype(f32)
    spread = jnp.concatenate([spread] * 3, 0)

    def spread_out(cells):
        return dot_cols(jnp.concatenate(split_exact(cells, 3), 0), spread)

    blocks = tokens // BLOCK
    zero_row = jnp.zeros((1, LANES), f32)
    eye = (row == lane).astype(f32)
    sizes = []
    size = 1
    while size < tokens:
        sizes.append(size)
        size *= 2

    def level_mask(k):
        return ((row >> (k + 1)) == (lane >> (k + 1))) & ((row >> k) != (lane >> k))

    ways = [[] for _ in range(per)]
    for d in range(2):
        lat_mask = head0 if d == 0 else ~head0
        lat_d = jnp.where(lat_mask, lat_ref[0].astype(f32), 0.0)
        lat_r = jnp.where(lat_mask, lat_ref[1].astype(f32), 0.0)
        pre = dbias_ref[d : d + 1, lanes] + dot(lat_d, draise_ref[:, lanes])
        velocity = jax.nn.sigmoid(pre) * 0.6065306597126334
        ld = -velocity * spread_out(tempo_ref[d]) + spread_out(extra_ref[d])
        rates = jax.nn.sigmoid(rbias_ref[d : d + 1, lanes] + dot(lat_r, rraise_ref[:, lanes]))
        upto = (lane <= row) if d == 0 else (lane >= row)
        strict = (lane < row) if d == 0 else (lane > row)
        tri = upto.astype(f32).astype(bf16)
        inners = dot(
            jnp.concatenate([tri, tri], 1), jnp.concatenate(split_exact(ld, 2), 0)
        )
        for j in range(per):
            inner = cut(inners, j)
            excl = inner - cut(ld, j)
            unit, query_in = units[j], cut(rf, j)
            removal = unit * cut(rates, j)
            written = cut(kf, j) * cut(rates, j)
            grams = []
            for i in range(blocks):
                lo, hi = i * BLOCK, (i + 1) * BLOCK
                if d == 0:
                    base = inner[lo - 1 : lo] if i > 0 else zero_row
                    live = slice(0, hi)
                else:
                    base = inner[hi : hi + 1] if i < blocks - 1 else zero_row
                    live = slice(lo, tokens)
                ahead = unit[lo:hi] * jnp.exp(excl[lo:hi] - base)
                query = query_in[lo:hi] * jnp.exp(inner[lo:hi] - base)
                grow = jnp.exp(jnp.minimum(base - inner[live], 80.0))
                rest = tokens - grow.shape[0]

                def filled(cells):
                    cells = cells.astype(bf16)
                    if not rest:
                        return cells
                    empty = jnp.zeros((rest, LANES), bf16)
                    return jnp.concatenate([cells, empty] if d == 0 else [empty, cells], 0)

                right = jnp.concatenate(
                    [filled(removal[live] * grow), filled(written[live] * grow)], 0
                )
                h0 = head0[lo:hi]
                left = jnp.concatenate(
                    [
                        jnp.where(h0, ahead, 0.0),
                        jnp.where(h0, 0.0, ahead),
                        jnp.where(h0, query, 0.0),
                        jnp.where(h0, 0.0, query),
                    ],
                    0,
                )
                grams.append(dot_rows(left, right))

            def gathered(place, at, mask):
                rows = jnp.concatenate(
                    [
                        gram[place * BLOCK : (place + 1) * BLOCK, at * tokens : (at + 1) * tokens]
                        for gram in grams
                    ],
                    0,
                )
                return jnp.where(mask, rows, 0.0)

            way = dict(inner=inner, excl=excl, removal=removal, written=written)
            way["link"] = [gathered(h, 0, strict) for h in range(2)]
            way["write"] = [gathered(h, 1, strict).astype(bf16) for h in range(2)]
            way["read"] = [gathered(2 + h, 0, upto).astype(bf16) for h in range(2)]
            way["read_write"] = [gathered(2 + h, 1, upto).astype(bf16) for h in range(2)]
            ways[j].append(way)

    links = [link for j in range(per) for way in ways[j] for link in way["link"]]
    mask = level_mask(0)
    inverses = [(eye - jnp.where(mask, a, 0.0)).astype(bf16) for a in links]
    links = [a.astype(bf16) for a in links]

    def products(lefts, rights):
        out = []
        for i in range(0, len(lefts), 2):
            result = dot(
                jnp.concatenate(lefts[i : i + 2], 1),
                jnp.concatenate(
                    [
                        jnp.concatenate([rights[i], blank], 1),
                        jnp.concatenate([blank, rights[i + 1]], 1),
                    ],
                    0,
                ),
            ).astype(bf16)
            out += [cut(result, 0), cut(result, 1)]
        return out

    for k in range(1, len(sizes)):
        mask = level_mask(k).astype(f32).astype(bf16)
        firsts = products(inverses, [a * mask for a in links])
        steps = products(firsts, inverses)
        inverses = [t - u for t, u in zip(inverses, steps)]

    block_diag = (row < HEAD) == head0
    for j in range(per):
        pair = g * per + j
        vj = cut(value, j)
        stacked = both_heads(vj)
        sums = dot(
            jnp.concatenate(
                [
                    jnp.concatenate(way[name], 1)
                    for way in ways[j]
                    for name in ("write", "read_write")
                ],
                0,
            ),
            stacked,
        )
        local = sums[tokens : 2 * tokens] + sums[3 * tokens :]
        for d, way in enumerate(ways[j]):
            inner, excl = way["inner"], way["excl"]
            last = inner[tokens - 1 : tokens] if d == 0 else inner[0:1]
            ahead = units[j] * jnp.exp(excl)
            query = cut(rf, j) * jnp.exp(inner)
            tail = jnp.exp(last - inner)
            base = sums[2 * d * tokens : (2 * d + 1) * tokens]
            rhs = jnp.concatenate([ahead.astype(bf16), base.astype(bf16)], 1)
            at = 4 * j + 2 * d
            solved = -dot(jnp.concatenate(inverses[at : at + 2], 1), rows_for_heads(rhs))
            solved = solved.astype(bf16)
            pull_map, pull_base = cut(solved, 0), cut(solved, 1)
            remove_tail = (way["removal"] * tail).astype(bf16)
            write_tail = (way["written"] * tail).astype(bf16)
            seen = dot(jnp.concatenate(way["read"], 1), rows_for_heads(solved))
            query_ref[d, :, pair * LANES : (pair + 1) * LANES] = (query + cut(seen, 0)).astype(bf16)
            local = local + cut(seen, 1)
            transfer = (
                jnp.where(block_diag, dot_cols(pull_map, remove_tail), 0.0) + eye * jnp.exp(last)
            )
            transfer_ref[d, pair] = transfer.astype(bf16)
            carried = dot_cols(
                jnp.concatenate([pull_base, vj], 0),
                jnp.concatenate([remove_tail, write_tail], 0),
            )
            carried = jnp.where(block_diag, carried, 0.0)
            carried_ref[d, pair] = carried[:HEAD] + carried[HEAD:]
        local_ref[:, pair * LANES : (pair + 1) * LANES] = local


def layer_kernel(
    nsp,
    nfs,
    ntp,
    x_ref,
    in_gain_ref,
    wk_hbm,
    wr_hbm,
    wv_hbm,
    wi_hbm,
    dl_hbm,
    rl_hbm,
    draise_ref,
    dbias_ref,
    rraise_ref,
    rbias_ref,
    tempo_ref,
    extra_ref,
    mix_hbm,
    gain_ref,
    wa_hbm,
    wp_hbm,
    out_ref,
    wk_ref,
    wr_ref,
    wv_ref,
    wi_ref,
    dl_ref,
    rl_ref,
    mix_ref,
    wa_ref,
    wp_ref,
    loaded,
    mine,
    cells,
    part,
    pool_part,
    onward,
    pool_onward,
    landed,
    pool_landed,
    joined,
    pool_joined,
    xs,
    xr,
    ps,
    pr,
    qs,
    qr,
    lat_ref,
    pool_ref,
    query_ref,
    local_ref,
    transfer_ref,
    carried_ref,
    edge,
    halo,
    incoming,
    leaving,
    act,
    tsend,
    trecv,
    sums_ref,
    osend,
    orecv,
    hs,
    hr,
    ss,
    sr,
    gs,
    gr,
    ts,
    tr,
    os,
    orr,
):
    z = lax.axis_index("sp")
    me = lax.axis_index("fs")
    core = lax.axis_index("tp")
    tokens, channels = local_ref.shape
    half_rows = tokens // ntp
    has_prev = z > 0
    has_next = z < nsp - 1
    prev = jnp.maximum(z - 1, 0)
    after = jnp.minimum(z + 1, nsp - 1)

    barrier = pltpu.get_barrier_semaphore()
    for d in range(1, nfs):
        greet(barrier, "fs", flipped(me, d))
    for d in range(1, ntp):
        greet(barrier, "tp", lax.rem(core + d, ntp))
    pl.when(has_prev)(lambda: greet(barrier, "sp", prev))
    pl.when(has_next)(lambda: greet(barrier, "sp", after))
    count = nfs + ntp - 2 + jnp.where(has_prev, 1, 0) + jnp.where(has_next, 1, 0)
    sources = (dl_hbm, rl_hbm, wk_hbm, wr_hbm, wv_hbm, wi_hbm, mix_hbm, wa_hbm, wp_hbm)
    targets = (dl_ref, rl_ref, wk_ref, wr_ref, wv_ref, wi_ref, mix_ref, wa_ref, wp_ref)
    loads = [
        pltpu.make_async_copy(source, target, loaded.at[i])
        for i, (source, target) in enumerate(zip(sources, targets))
    ]
    for load in loads:
        load.start()
    def state_copy(d, g):
        return remote(
            leaving.at[d, g],
            incoming.at[d, g],
            ss.at[d, g],
            sr.at[d, g],
            "sp",
            after if d == 0 else prev,
        )

    halo_copies = [
        remote(edge.at[1], halo.at[0], hs.at[0], hr.at[0], "sp", after),
        remote(edge.at[0], halo.at[1], hs.at[1], hr.at[1], "sp", prev),
    ]
    sends = [has_next, has_prev]
    takes = [has_prev, has_next]
    groups = incoming.shape[1]
    per = incoming.shape[2]

    def mix_step(g, *operands):
        mix_group(g, *operands)
        for d in range(2):

            @pl.when(jnp.logical_not(takes[d]))
            def _():
                incoming[d, g] = jnp.zeros_like(incoming[d, g])
                for j in range(per):
                    leaving[d, g, j] = carried_ref[d, g * per + j].astype(bf16)
                pl.when(sends[d])(lambda: state_copy(d, g).start())

    def relay(d, g):
        @pl.when(takes[d])
        def _():
            state_copy(d, g).wait_recv()

            @pl.when(sends[d])
            def _():
                for j in range(per):
                    p = g * per + j
                    leaving[d, g, j] = (
                        dot(incoming[d, g, j], transfer_ref[d, p]) + carried_ref[d, p]
                    ).astype(bf16)
                state_copy(d, g).start()

    early = 2 * z < nsp

    def relays(near, g):
        @pl.when(early)
        def _():
            relay(0 if near else 1, g)

        @pl.when(jnp.logical_not(early))
        def _():
            relay(1 if near else 0, g)

    finish_front = front_part(
        nfs,
        x_ref,
        in_gain_ref,
        (wk_ref, wr_ref, wv_ref, wi_ref),
        (dl_ref, rl_ref),
        loads[:6],
        pool_ref,
        lat_ref,
        mine,
        cells,
        part,
        pool_part,
        onward,
        pool_onward,
        landed,
        pool_landed,
        joined,
        pool_joined,
        xs,
        xr,
        ps,
        pr,
        qs,
        qr,
        count,
        lambda g, key, receptance, value: mix_step(
            g,
            key,
            receptance,
            value,
            lat_ref,
            draise_ref,
            dbias_ref,
            rraise_ref,
            rbias_ref,
            tempo_ref,
            extra_ref,
            query_ref,
            local_ref,
            transfer_ref,
            carried_ref,
        ),
    )
    for load in loads[6:]:
        load.wait()
    with jax.named_scope("relayA0"):
        relays(True, 0)
    edge[0] = pool_ref[:HALO]
    edge[1] = pool_ref[tokens - HALO :]
    for d in range(2):
        pl.when(sends[d])(lambda: halo_copies[d].start())
    for g in range(1, groups):
        with jax.named_scope(f"relayA{g}"):
            relays(True, g)
    with jax.named_scope("halo"):
        for d in range(2):

            @pl.when(takes[d])
            def _():
                halo_copies[d].wait_recv()

            @pl.when(jnp.logical_not(takes[d]))
            def _():
                halo[d] = jnp.zeros_like(halo[d])

    span = tokens + 2 * HALO
    rim = jnp.concatenate([halo[0], pool_ref[...], halo[1]], 0)
    here = lax.broadcasted_iota(jnp.int32, (tokens, span), 0)
    there = lax.broadcasted_iota(jnp.int32, (tokens, span), 1) - HALO
    position = z * tokens + lax.broadcasted_iota(jnp.int32, (tokens, GROUP_WIDTH), 0)
    length = tokens * nsp
    groups_here = channels // GROUP_WIDTH
    for member in range(groups_here):
        cols = slice(member * GROUP_WIDTH, (member + 1) * GROUP_WIDTH)
        reach = jnp.left_shift(1, core * groups_here + member)
        window = jnp.where((there >= here - reach) & (there < here + reach), 1.0, 0.0)
        total = dot(window, rim[:, cols])
        size = (
            jnp.minimum(position + reach, length) - jnp.maximum(position - reach, 0)
        ).astype(f32)
        diff = (total / size - pool_ref[:, cols].astype(f32)).astype(bf16)
        act[me, 0, :, cols] = dot(diff, mix_ref[member]).astype(bf16)
    order = list(range(nfs - 1, 0, -1))
    shares = []
    for d in order:
        peer = flipped(me, d)
        copy = remote(act.at[me, 0], act.at[me, 0], gs.at[d, 0], gr.at[d, 0], "fs", peer)
        copy.start()
        shares.append(copy)

    head0 = lax.broadcasted_iota(jnp.int32, (tokens, LANES), 1) < HEAD
    top0 = lax.broadcasted_iota(jnp.int32, (HEAD, LANES), 1) < HEAD

    def head_mean(values):
        low = jnp.sum(jnp.where(head0, values, 0.0), axis=-1, keepdims=True)
        high = jnp.sum(jnp.where(head0, 0.0, values), axis=-1, keepdims=True)
        return jnp.where(head0, low, high) * (1.0 / HEAD)

    for g in range(groups):
        with jax.named_scope(f"relayB{g}"):
            relays(False, g)
        with jax.named_scope(f"readout{g}"):
            for j in range(per):
                p = g * per + j
                lanes = slice(p * LANES, (p + 1) * LANES)
                readout = local_ref[:, lanes]
                for d in range(2):
                    state = incoming[d, g, j].astype(f32)
                    whole = jnp.concatenate(
                        [jnp.where(top0, state, 0.0), jnp.where(top0, 0.0, state)], 0
                    )
                    readout = readout + dot_rows(query_ref[d, :, lanes], whole)
                centred = readout - head_mean(readout)
                scaled = centred * lax.rsqrt(head_mean(centred * centred) + head_eps)
                act[me, 1, :, lanes] = (
                    scaled * gain_ref[lanes].astype(f32).reshape(1, -1)
                ).astype(bf16)
            cols = pl.ds(g * per * LANES, per * LANES)
            for d in order:
                copy = remote(
                    act.at[me, 1, :, cols],
                    act.at[me, 1, :, cols],
                    gs.at[d, 1 + g],
                    gr.at[d, 1 + g],
                    "fs",
                    flipped(me, d),
                )
                copy.start()
                shares.append(copy)

    other = lax.rem(core + 1, ntp)
    mine_at = pl.multiple_of(core * half_rows, half_rows)
    other_at = pl.multiple_of(other * half_rows, half_rows)

    def product(seq):
        return dot_rows(act[seq, 1], wa_ref[...]) + dot_rows(act[seq, 0], wp_ref[...])

    returns = []
    swaps = []
    turns = [0] + order
    for d in turns:
        seq = flipped(me, d)
        if d:
            with jax.named_scope("actwait"):
                for copy, at in zip(shares, order * (1 + groups)):
                    if at == d:
                        copy.wait_recv()
        with jax.named_scope("prod"):
            sums_ref[...] = product(seq)
            tsend[d] = sums_ref[pl.ds(other_at, half_rows)].astype(bf16)
        swap = remote(tsend.at[d], trecv.at[d], ts.at[d], tr.at[d], "tp", other)
        swap.start()
        swaps.append(swap)
        kept = sums_ref[pl.ds(mine_at, half_rows)]
        with jax.named_scope("swapwait"):
            swap.wait_recv()
        whole = (kept + trecv[d].astype(f32)).astype(bf16)
        if d:
            osend[d] = whole
            copy = remote(osend.at[d], orecv.at[me], os.at[d], orr.at[d], "fs", seq)
            copy.start()
            returns.append(copy)
        else:
            orecv[me] = whole
    with jax.named_scope("retwait"):
        for copy in returns:
            copy.wait_recv()
    for j in range(nfs):
        out_ref[0, :, j * channels : (j + 1) * channels] = orecv[j]
    for copy in shares + swaps + returns:
        copy.wait_send()
    for d in range(2):

        @pl.when(sends[d])
        def _():
            for g in range(groups):
                state_copy(d, g).wait_send()
            halo_copies[d].wait_send()
    finish_front()


def shards(
    inputs,
    input_norm_gain,
    receptance_matrix,
    key_matrix,
    value_matrix,
    pooling_input_weight,
    decay_lower_matrix,
    decay_raise_matrix,
    decay_offset_bias,
    removal_lower_matrix,
    removal_raise_matrix,
    removal_rate_bias,
    tempo_scale,
    sudden_decay_extra,
    head_norm_gain,
    group_mixing_weight,
    attention_output_matrix,
    pooling_output_matrix,
):
    nsp, nfs, ntp = lax.axis_size("sp"), lax.axis_size("fs"), lax.axis_size("tp")
    _, tokens, features = inputs.shape
    depth, channels = key_matrix.shape
    pairs = channels // LANES
    groups = pairs // PER
    wide = PER * LANES
    dma = pltpu.SemaphoreType.DMA
    rank = decay_lower_matrix.shape[1]
    rank2 = decay_raise_matrix.shape[0] * decay_raise_matrix.shape[1]
    anywhere = pl.BlockSpec(memory_space=pl.ANY)
    half = (nfs, tokens // ntp, depth)
    return pl.pallas_call(
        functools.partial(layer_kernel, nsp, nfs, ntp),
        out_shape=jax.ShapeDtypeStruct((1, tokens // ntp, features), bf16),
        in_specs=[VMEM] * 2
        + [anywhere] * 6
        + [VMEM] * 6
        + [anywhere, VMEM, anywhere, anywhere],
        out_specs=VMEM,
        scratch_shapes=[pltpu.VMEM((depth, channels), bf16)] * 4
        + [
            pltpu.VMEM((features, rank), bf16),
            pltpu.VMEM((features, rank), bf16),
            pltpu.VMEM(group_mixing_weight.shape, bf16),
            pltpu.VMEM(attention_output_matrix.shape, bf16),
            pltpu.VMEM(pooling_output_matrix.shape, bf16),
            dma((9,)),
            pltpu.VMEM((nfs, tokens, depth), bf16),
            pltpu.VMEM((nfs, tokens, depth), bf16),
            pltpu.VMEM((groups, 2, 3, tokens, wide), bf16),
            pltpu.VMEM((2, tokens, channels), bf16),
            pltpu.VMEM((groups, 3, tokens, wide), bf16),
            pltpu.VMEM((tokens, channels), bf16),
            pltpu.VMEM((groups, 2, 3, tokens, wide), bf16),
            pltpu.VMEM((2, tokens, channels), bf16),
            pltpu.VMEM((groups, 3, tokens, wide), bf16),
            pltpu.VMEM((tokens, channels), bf16),
            dma((nfs, ntp)),
            dma((nfs, ntp)),
            dma((groups + 1, 2)),
            dma((groups + 1, 2)),
            dma((groups + 1,)),
            dma((groups + 1,)),
            pltpu.VMEM((2, tokens, rank), bf16),
            pltpu.VMEM((tokens, channels), bf16),
            pltpu.VMEM((2, tokens, channels), bf16),
            pltpu.VMEM((tokens, channels), f32),
            pltpu.VMEM((2, pairs, LANES, LANES), bf16),
            pltpu.VMEM((2, pairs, HEAD, LANES), f32),
            pltpu.VMEM((2, HALO, channels), bf16),
            pltpu.VMEM((2, HALO, channels), bf16),
            pltpu.VMEM((2, groups, PER, HEAD, LANES), bf16),
            pltpu.VMEM((2, groups, PER, HEAD, LANES), bf16),
            pltpu.VMEM((nfs, 2, tokens, channels), bf16),
            pltpu.VMEM(half, bf16),
            pltpu.VMEM(half, bf16),
            pltpu.VMEM((tokens, depth), f32),
            pltpu.VMEM(half, bf16),
            pltpu.VMEM(half, bf16),
            dma((2,)),
            dma((2,)),
            dma((2, groups)),
            dma((2, groups)),
            dma((nfs, 1 + groups)),
            dma((nfs, 1 + groups)),
            dma((nfs,)),
            dma((nfs,)),
            dma((nfs,)),
            dma((nfs,)),
        ],
        compiler_params=pltpu.CompilerParams(
            collective_id=0, has_side_effects=True, vmem_limit_bytes=60 * 1024 * 1024
        ),
        name="layer",
    )(
        inputs,
        input_norm_gain,
        key_matrix,
        receptance_matrix,
        value_matrix,
        pooling_input_weight,
        decay_lower_matrix,
        removal_lower_matrix,
        decay_raise_matrix.reshape(rank2, channels),
        decay_offset_bias,
        removal_raise_matrix.reshape(rank2, channels),
        removal_rate_bias,
        tempo_scale[0],
        sudden_decay_extra[0],
        group_mixing_weight,
        head_norm_gain,
        attention_output_matrix,
        pooling_output_matrix,
    )


def solution(mesh):
    in_specs = (
        P("fs", "sp", None),
        P(),
        P("fs", "tp"),
        P("fs", "tp"),
        P("fs", "tp"),
        P("fs", "tp"),
        P(),
        P(None, None, "tp"),
        P(None, "tp"),
        P(),
        P(None, None, "tp"),
        P(None, "tp"),
        P("fs", None, "tp", "sp"),
        P("fs", None, "tp", "sp"),
        P("tp"),
        P("tp", None, None),
        P("fs", "tp"),
        P("fs", "tp"),
    )
    out_specs = P("fs", ("sp", "tp"), None)
    return jax.shard_map(shards, mesh=mesh, in_specs=in_specs, out_specs=out_specs, check_vma=False)
```

time: 64.9 us -> 58.4 us (0.90)
  Pallas kernels: 63.1 us -> 56.6 us
    pallas_call x1, Pallas kernels: 63.1 us -> 56.6 us  [shards(): pl.pallas_call(functools.partial(layer_kernel, nsp, nfs, ntp), out_shape=...]
where the time goes in v1:
time: 58.4 us; the launch traced here: 58.3 us
  Pallas kernels  56.6 us (97%)
  local copies, waits for them, and re-layouts  1.67 us (3%)
    pallas_call x1, Pallas kernels, shards(): pl.pallas_call(functools.partial(layer_kernel, nsp, nfs, ntp), out_shape=...  56.6 us
    unnamed x1, local copies, waits for them, and re-layouts  1.67 us

profile of v1, /device:TPU:0, one launch (start us, length us, event | category | flops | bytes accessed | tf_op | source)
XLA Modules:
  0.0 58.3 jit_solution(14410755445558143928)
XLA Ops:
  0.0 56.6 %layer.1 = bf16[1,64,2048]{2,1,0:T(8,128)(2,1)} custom-call(bf16[1,128,2048]{2,1,0:T(8,128)(2,1)} %x_ref.1, bf16[2048]{0:T(1024)(128)(2,1)} %in_gain_ref.1, bf16[512,512]{1,0:T(8,128)(2,1)} %wk_hbm.1, bf16[512,512]{1,0:T(8,128)(2,1)} %wr_hbm.1, bf16[512,512]{1,0:T(8,128)(2,1)} %wv_hbm.1, bf16[512,512]{1,0:T(8,128)(2,1)} %wi_hbm.1, bf16[2048,128]{1,0:T(8,128)(2,1)} %dl_hbm.1, ...), custom_call_target="tpu_custom_call" | custom-call | tf_op jit(solution)/shard_map/layer/pallas_call | solution.py:857
  56.6 1.7 %copy.20 = bf16[1,64,2048]{2,1,0:T(8,128)(2,1)} copy(bf16[1,64,2048]{2,1,0:T(8,128)(2,1)} %layer.1) | data formatting | bytes 524288

commit v2 on v1

v2 whole, which is shorter than its diff:
```python
import functools

import jax
import jax.numpy as jnp
from jax import lax
from jax.experimental import pallas as pl
from jax.experimental.pallas import tpu as pltpu
from jax.sharding import PartitionSpec as P

HEAD = 64
GROUP_WIDTH = 256
LANES = 128
BLOCK = 16
HALO = 16

norm_eps = 1e-06
head_eps = 0.00064
unit_eps = 1e-06
f32 = jnp.float32
bf16 = jnp.bfloat16
VMEM = pl.BlockSpec(memory_space=pltpu.VMEM)


def dot(left, right):
    return jnp.dot(left.astype(bf16), right.astype(bf16), preferred_element_type=f32)


def dot_general(left, right, dims):
    return lax.dot_general(
        left.astype(bf16), right.astype(bf16), (dims, ((), ())), preferred_element_type=f32
    )


def dot_rows(left, right):
    return dot_general(left, right, ((1,), (1,)))


def dot_cols(left, right):
    return dot_general(left, right, ((0,), (0,)))


def split_exact(cells, pieces):
    parts = []
    for _ in range(pieces - 1):
        high = cells.astype(bf16).astype(f32)
        parts.append(high)
        cells = cells - high
    return parts + [cells]


def remote(src, dst, send, recv, axis, peer):
    return pltpu.make_async_remote_copy(
        src_ref=src,
        dst_ref=dst,
        send_sem=send,
        recv_sem=recv,
        device_id={axis: peer},
        device_id_type=pl.DeviceIdType.MESH,
    )


def greet(barrier, axis, peer):
    pl.semaphore_signal(
        barrier, inc=1, device_id={axis: peer}, device_id_type=pl.DeviceIdType.MESH
    )


def flipped(at, bits):
    moved = at
    bit = 1
    while bit <= bits:
        if bits & bit:
            moved = moved + bit - 2 * bit * lax.rem(at // bit, 2)
        bit *= 2
    return moved


def front_part(
    n,
    x_ref,
    gain_ref,
    weights,
    lowers,
    loads,
    pool_ref,
    lat_ref,
    mine,
    cells,
    part,
    pool_part,
    onward,
    pool_onward,
    landed,
    pool_landed,
    joined,
    pool_joined,
    xs,
    xr,
    ps,
    pr,
    qs,
    qr,
    count,
    greet_line,
    meet_line,
    prepare,
    mix_group,
):
    me = lax.axis_index("fs")
    core, ntp = lax.axis_index("tp"), lax.axis_size("tp")
    width = x_ref.shape[2] // n
    plan = group_plan(part.shape[1])
    groups = len(plan)
    with jax.named_scope("xload"):
        for load in loads[:2]:
            load.wait()
    x = x_ref[0].astype(f32)
    with jax.named_scope("norm"):
        normed = (
            x
            * lax.rsqrt(jnp.mean(x * x, axis=-1, keepdims=True) + norm_eps)
            * gain_ref[...].astype(f32).reshape(1, -1)
        ).astype(bf16)
        for j in range(n):
            mine[j] = normed[:, j * width : (j + 1) * width]
    order = list(range(n - 1, 0, -1))
    lead = core == ntp - 1

    def row_copy(d):
        peer = flipped(me, d)
        return remote(mine.at[peer], cells.at[me], xs.at[d, 0], xr.at[d, 0], "fs", peer)

    def pass_copy(d, e):
        at = cells.at[flipped(me, d)]
        return remote(at, at, xs.at[d, 1 + e], xr.at[d, 1], "tp", e)

    with jax.named_scope("barrier"):

        @pl.when(lead)
        def _():
            pl.semaphore_wait(pltpu.get_barrier_semaphore(), count)
            for d in order:
                row_copy(d).start()

    with jax.named_scope("latent"):
        for load in loads[2:4]:
            load.wait()
        dl_ref, rl_ref = lowers
        decay = jnp.zeros((x.shape[0], dl_ref.shape[1]), f32)
        rate = jnp.zeros((x.shape[0], rl_ref.shape[1]), f32)
        for j in range(n):
            block = mine[j]
            decay = decay + dot(block, dl_ref[j * width : (j + 1) * width])
            rate = rate + dot(block, rl_ref[j * width : (j + 1) * width])
        lat_ref[0] = jnp.tanh(decay.astype(bf16).astype(f32)).astype(bf16)
        lat_ref[1] = rate.astype(bf16)
        for load in loads[4:]:
            load.wait()
    with jax.named_scope("xwait"):
        @pl.when(lead)
        def _():
            for d in order:
                row_copy(d).wait_recv()
                for e in range(ntp - 1):
                    pass_copy(d, e).start()

        @pl.when(jnp.logical_not(lead))
        def _():
            for d in order:
                pass_copy(d, 0).wait_recv()

        greet_line()

    first, second, across = routes(me, n, core)
    targets = (first, across)

    def span_of(g):
        at, count = plan[g]
        return pl.ds(at, count)

    def first_copy(g, slot):
        return remote(
            part.at[slot, span_of(g)],
            landed.at[slot, span_of(g)],
            ps.at[g, slot],
            pr.at[g, slot],
            "fs",
            first,
        )

    def first_pool(slot):
        return remote(
            pool_part.at[slot],
            pool_landed.at[slot],
            ps.at[groups, slot],
            pr.at[groups, slot],
            "fs",
            first,
        )

    def second_copy(g):
        return remote(
            onward.at[span_of(g)], joined.at[span_of(g)], qs.at[g], qr.at[g], "fs", second
        )

    second_pool = remote(
        pool_onward, pool_joined, qs.at[groups], qr.at[groups], "fs", second
    )

    def piece(m, g):
        at, count = plan[g]
        return weights[m][:, at * LANES : (at + count) * LANES]

    def beside(ref, g, m):
        at, count = plan[g]
        return jnp.concatenate([ref[p, m] for p in range(at, at + count)], 1).astype(f32)

    def keep(ref, g, m, cells):
        at, count = plan[g]
        for j in range(count):
            ref[at + j, m] = cells[:, j * LANES : (j + 1) * LANES].astype(bf16)

    with jax.named_scope("partials"):
        for g in range(groups):
            for slot in (1, 0):
                for m in range(3):
                    keep(part.at[slot], g, m, dot(cells[targets[slot]], piece(m, g)))
                first_copy(g, slot).start()

    def forward(g):
        with jax.named_scope(f"fwd{g}"):
            first_copy(g, 1).wait_recv()
            for m in range(3):
                keep(
                    onward, g, m, dot(cells[second], piece(m, g)) + beside(landed.at[1], g, m)
                )
            second_copy(g).start()

    def begin_pool():
        with jax.named_scope("beginpool"):
            for slot in (1, 0):
                pool_part[slot] = dot(cells[targets[slot]], weights[3][...]).astype(bf16)
                first_pool(slot).start()

    def forward_pool():
        with jax.named_scope("fwdpool"):
            first_pool(1).wait_recv()
            pool_onward[...] = (
                dot(cells[second], weights[3][...]) + pool_landed[1].astype(f32)
            ).astype(bf16)
            second_pool.start()

    def prep(g):
        with jax.named_scope(f"prep{g}"):
            prepare(g)

    def settle(g):
        with jax.named_scope(f"settle{g}"):
            first_copy(g, 0).wait_recv()
            second_copy(g).wait_recv()
        with jax.named_scope(f"mix{g}"):
            owned = [
                (
                    dot(mine[me], piece(m, g))
                    + beside(landed.at[0], g, m)
                    + beside(joined, g, m)
                ).astype(bf16)
                for m in range(3)
            ]
            mix_group(g, *owned)

    prep(0)
    forward(0)
    prep(1)
    forward(1)
    prep(2)
    meet_line()
    settle(0)
    forward(2)
    begin_pool()
    settle(1)
    forward_pool()
    settle(2)
    def settle_pool():
        with jax.named_scope("poolin"):
            first_pool(0).wait_recv()
            second_pool.wait_recv()
            pool_ref[...] = (
                dot(mine[me], weights[3][...])
                + pool_landed[0].astype(f32)
                + pool_joined[...].astype(f32)
            ).astype(bf16)

    def finish():
        @pl.when(lead)
        def _():
            for d in order:
                row_copy(d).wait_send()
                for e in range(ntp - 1):
                    pass_copy(d, e).wait_send()

        for g in range(groups):
            for slot in (1, 0):
                first_copy(g, slot).wait_send()
            second_copy(g).wait_send()
        for slot in (1, 0):
            first_pool(slot).wait_send()
        second_pool.wait_send()

    return settle_pool, finish


def group_plan(pairs):
    quarter = pairs // 4
    return [(0, quarter), (quarter, pairs - 2 * quarter), (pairs - quarter, quarter)]


def routes(me, n, core):
    low, high = flipped(me, 1), flipped(me, n // 2)
    odd = lax.rem(core, 2)
    return low + odd * (high - low), high + odd * (low - high), flipped(me, n // 2 + 1)


def cut(cells, j):
    return cells[:, j * LANES : (j + 1) * LANES]


def live_rows(d, i, tokens):
    return slice(0, (i + 1) * BLOCK) if d == 0 else slice(i * BLOCK, tokens)


def prepare_group(
    start,
    per,
    lat_ref,
    draise_ref,
    dbias_ref,
    rraise_ref,
    rbias_ref,
    tempo_ref,
    extra_ref,
    fade_ref,
    grow_ref,
):
    tokens = lat_ref.shape[1]
    wide = per * LANES
    lanes = slice(start * LANES, start * LANES + wide)
    lane = lax.broadcasted_iota(jnp.int32, (tokens, LANES), 1)
    row = lax.broadcasted_iota(jnp.int32, (tokens, LANES), 0)
    head0 = lane < HEAD
    heads = tempo_ref.shape[1]
    spread = (
        lax.broadcasted_iota(jnp.int32, (heads, wide), 0)
        == 2 * start + lax.broadcasted_iota(jnp.int32, (heads, wide), 1) // HEAD
    ).astype(f32)
    spread = jnp.concatenate([spread] * 3, 0)

    def spread_out(cells):
        return dot_cols(jnp.concatenate(split_exact(cells, 3), 0), spread)

    blocks = tokens // BLOCK
    zero_row = jnp.zeros((1, wide), f32)
    for d in range(2):
        lat_mask = head0 if d == 0 else ~head0
        lat_d = jnp.where(lat_mask, lat_ref[0].astype(f32), 0.0)
        lat_r = jnp.where(lat_mask, lat_ref[1].astype(f32), 0.0)
        pre = dbias_ref[d : d + 1, lanes] + dot(lat_d, draise_ref[:, lanes])
        velocity = jax.nn.sigmoid(pre) * 0.6065306597126334
        ld = -velocity * spread_out(tempo_ref[d]) + spread_out(extra_ref[d])
        rate = jax.nn.sigmoid(rbias_ref[d : d + 1, lanes] + dot(lat_r, rraise_ref[:, lanes]))
        upto = (lane <= row) if d == 0 else (lane >= row)
        tri = upto.astype(f32).astype(bf16)
        inner = dot(jnp.concatenate([tri, tri], 1), jnp.concatenate(split_exact(ld, 2), 0))
        excl = inner - ld
        last = inner[tokens - 1 : tokens] if d == 0 else inner[0:1]
        fade_ref[d, 0, :, lanes] = jnp.exp(excl)
        fade_ref[d, 1, :, lanes] = jnp.exp(inner)
        fade_ref[d, 2, :, lanes] = jnp.exp(last - inner) * rate
        for i in range(blocks):
            lo, hi = i * BLOCK, (i + 1) * BLOCK
            if d == 0:
                base = inner[lo - 1 : lo] if i > 0 else zero_row
            else:
                base = inner[hi : hi + 1] if i < blocks - 1 else zero_row
            live = live_rows(d, i, tokens)
            fade_ref[d, 3, lo:hi, lanes] = jnp.exp(excl[lo:hi] - base)
            fade_ref[d, 4, lo:hi, lanes] = jnp.exp(inner[lo:hi] - base)
            grow = jnp.exp(jnp.minimum(base - inner[live], 80.0))
            grow_ref[d, i, live, lanes] = grow * rate[live]


def mix_group(
    start,
    key,
    receptance,
    value,
    fade_ref,
    grow_ref,
    query_ref,
    local_ref,
    transfer_ref,
    carried_ref,
):
    tokens, wide = key.shape
    per = wide // LANES
    kf = key.astype(f32)
    rf = receptance.astype(f32)
    lane = lax.broadcasted_iota(jnp.int32, (tokens, LANES), 1)
    row = lax.broadcasted_iota(jnp.int32, (tokens, LANES), 0)
    head0 = lane < HEAD
    only = [head0.astype(f32).astype(bf16), (~head0).astype(f32).astype(bf16)]
    blank = jnp.zeros((tokens, LANES), bf16)

    def both_heads(cells):
        return jnp.concatenate([cells * only[0], cells * only[1]], 0)

    def rows_for_heads(cells):
        return jnp.concatenate(
            [jnp.concatenate([cut(cells, i) * o for i in range(cells.shape[1] // LANES)], 1) for o in only], 0
        )

    units = []
    for j in range(per):
        kj = cut(kf, j)
        k2 = kj * kj
        s0 = jnp.sum(jnp.where(head0, k2, 0.0), axis=-1, keepdims=True)
        s1 = jnp.sum(jnp.where(head0, 0.0, k2), axis=-1, keepdims=True)
        units.append(kj * lax.rsqrt(jnp.where(head0, s0, s1) + unit_eps))
    blocks = tokens // BLOCK
    eye = (row == lane).astype(f32)
    sizes = []
    size = 1
    while size < tokens:
        sizes.append(size)
        size *= 2

    def level_mask(k):
        return ((row >> (k + 1)) == (lane >> (k + 1))) & ((row >> k) != (lane >> k))

    ways = [[] for _ in range(per)]
    for d in range(2):
        upto = (lane <= row) if d == 0 else (lane >= row)
        strict = (lane < row) if d == 0 else (lane > row)
        for j in range(per):
            at = slice((start + j) * LANES, (start + j + 1) * LANES)
            unit, kj, rj = units[j], cut(kf, j), cut(rf, j)
            aheads = unit * fade_ref[d, 3, :, at]
            queries = rj * fade_ref[d, 4, :, at]
            firsts = [
                jnp.where(head0, aheads, 0.0).astype(bf16),
                jnp.where(head0, 0.0, aheads).astype(bf16),
                jnp.where(head0, queries, 0.0).astype(bf16),
                jnp.where(head0, 0.0, queries).astype(bf16),
            ]
            grams = []
            for i in range(blocks):
                lo, hi = i * BLOCK, (i + 1) * BLOCK
                live = live_rows(d, i, tokens)
                grow = grow_ref[d, i, live, at]
                rest = tokens - grow.shape[0]

                def filled(cells):
                    cells = cells.astype(bf16)
                    if not rest:
                        return cells
                    empty = jnp.zeros((rest, LANES), bf16)
                    return jnp.concatenate([cells, empty] if d == 0 else [empty, cells], 0)

                right = jnp.concatenate(
                    [filled(unit[live] * grow), filled(kj[live] * grow)], 0
                )
                grams.append(dot_rows(jnp.concatenate([f[lo:hi] for f in firsts], 0), right))

            def gathered(place, at, mask):
                rows = jnp.concatenate(
                    [
                        gram[place * BLOCK : (place + 1) * BLOCK, at * tokens : (at + 1) * tokens]
                        for gram in grams
                    ],
                    0,
                )
                return jnp.where(mask, rows, 0.0)

            way = dict()
            way["link"] = [gathered(h, 0, strict) for h in range(2)]
            way["write"] = [gathered(h, 1, strict).astype(bf16) for h in range(2)]
            way["read"] = [gathered(2 + h, 0, upto).astype(bf16) for h in range(2)]
            way["read_write"] = [gathered(2 + h, 1, upto).astype(bf16) for h in range(2)]
            ways[j].append(way)

    links = [link for j in range(per) for way in ways[j] for link in way["link"]]
    mask = level_mask(0)
    inverses = [(eye - jnp.where(mask, a, 0.0)).astype(bf16) for a in links]
    links = [a.astype(bf16) for a in links]

    def products(lefts, rights):
        out = []
        for i in range(0, len(lefts), 2):
            result = dot(
                jnp.concatenate(lefts[i : i + 2], 1),
                jnp.concatenate(
                    [
                        jnp.concatenate([rights[i], blank], 1),
                        jnp.concatenate([blank, rights[i + 1]], 1),
                    ],
                    0,
                ),
            ).astype(bf16)
            out += [cut(result, 0), cut(result, 1)]
        return out

    def level_bits(k):
        return level_mask(k).astype(f32).astype(bf16)

    for k in range(1, len(sizes), 2):
        if k + 1 == len(sizes):
            mask = level_bits(k)
            firsts = products(inverses, [a * mask for a in links])
            steps = products(firsts, inverses)
            inverses = [t - u for t, u in zip(inverses, steps)]
            continue
        mask = level_bits(k) + level_bits(k + 1)
        firsts = products(inverses, [a * mask for a in links])
        steps = products(firsts, inverses)
        squares = products(firsts, firsts)
        inverses = [t - u for t, u in zip(inverses, steps)]
        inverses = [t + u for t, u in zip(inverses, products(squares, inverses))]

    block_diag = (row < HEAD) == head0
    for j in range(per):
        pair = start + j
        vj = cut(value, j)
        stacked = both_heads(vj)
        sums = dot(
            jnp.concatenate(
                [
                    jnp.concatenate(way[name], 1)
                    for way in ways[j]
                    for name in ("write", "read_write")
                ],
                0,
            ),
            stacked,
        )
        local = sums[tokens : 2 * tokens] + sums[3 * tokens :]
        at = slice(pair * LANES, (pair + 1) * LANES)
        for d, way in enumerate(ways[j]):
            ahead = units[j] * fade_ref[d, 0, :, at]
            query = cut(rf, j) * fade_ref[d, 1, :, at]
            edge_row = tokens - 1 if d == 0 else 0
            last = fade_ref[d, 1, edge_row : edge_row + 1, at]
            base = sums[2 * d * tokens : (2 * d + 1) * tokens]
            rhs = jnp.concatenate([ahead.astype(bf16), base.astype(bf16)], 1)
            place = 4 * j + 2 * d
            solved = -dot(jnp.concatenate(inverses[place : place + 2], 1), rows_for_heads(rhs))
            solved = solved.astype(bf16)
            tail = fade_ref[d, 2, :, at]
            remove_tail = (units[j] * tail).astype(bf16)
            write_tail = (cut(kf, j) * tail).astype(bf16)
            seen = dot(jnp.concatenate(way["read"], 1), rows_for_heads(solved))
            query_ref[d, :, pair * LANES : (pair + 1) * LANES] = (query + cut(seen, 0)).astype(bf16)
            local = local + cut(seen, 1)
            onto = dot_cols(remove_tail, solved)
            transfer = jnp.where(block_diag, cut(onto, 0), 0.0) + eye * last
            transfer_ref[d, pair] = transfer.astype(bf16)
            carried = cut(onto, 1) + dot_cols(write_tail, vj)
            carried_ref[d, pair] = jnp.where(
                head0[:HEAD], carried[:HEAD], carried[HEAD:]
            )
        local_ref[:, pair * LANES : (pair + 1) * LANES] = local


def layer_kernel(
    nsp,
    nfs,
    ntp,
    x_hbm,
    in_gain_hbm,
    wk_hbm,
    wr_hbm,
    wv_hbm,
    wi_hbm,
    dl_hbm,
    rl_hbm,
    draise_hbm,
    dbias_hbm,
    rraise_hbm,
    rbias_hbm,
    tempo_hbm,
    extra_hbm,
    mix_hbm,
    gain_hbm,
    wa_hbm,
    wp_hbm,
    out_hbm,
    x_ref,
    in_gain_ref,
    draise_ref,
    dbias_ref,
    rraise_ref,
    rbias_ref,
    tempo_ref,
    extra_ref,
    gain_ref,
    wk_ref,
    wr_ref,
    wv_ref,
    wi_ref,
    dl_ref,
    rl_ref,
    mix_ref,
    wa_ref,
    wp_ref,
    loaded,
    mine,
    cells,
    part,
    pool_part,
    onward,
    pool_onward,
    landed,
    pool_landed,
    joined,
    pool_joined,
    xs,
    xr,
    ready,
    ps,
    pr,
    qs,
    qr,
    lat_ref,
    fade_ref,
    grow_ref,
    pool_ref,
    query_ref,
    local_ref,
    transfer_ref,
    carried_ref,
    edge,
    halo,
    incoming,
    leaving,
    near_state,
    near_map,
    skipped,
    onto_next,
    act,
    tsend,
    trecv,
    sums_ref,
    osend,
    hs,
    hr,
    ss,
    sr,
    gs,
    gr,
    ts,
    tr,
    os,
    orr,
):
    z = lax.axis_index("sp")
    me = lax.axis_index("fs")
    core = lax.axis_index("tp")
    tokens, channels = local_ref.shape
    depth = wa_ref.shape[0]
    half_rows = tokens // ntp
    has_prev = z > 0
    has_next = z < nsp - 1
    prev = jnp.maximum(z - 1, 0)
    after = jnp.minimum(z + 1, nsp - 1)
    prev2 = jnp.maximum(z - 2, 0)
    after2 = jnp.minimum(z + 2, nsp - 1)

    barrier = pltpu.get_barrier_semaphore()
    lead = core == ntp - 1

    @pl.when(lead)
    def _():
        for d in range(1, nfs):
            greet(barrier, "fs", flipped(me, d))

    @pl.when(jnp.logical_not(lead))
    def _():
        greet(barrier, "tp", ntp - 1)

    near = ((has_prev, prev), (has_next, after), (z > 1, prev2), (z < nsp - 2, after2))

    def greet_line():
        @pl.when(core == 0)
        def _():
            for there, peer in near:
                pl.when(there)(lambda: greet(barrier, "sp", peer))

    def meet_line():
        @pl.when(core == 0)
        def _():
            count = 0
            for there, _ in near:
                count = count + jnp.where(there, 1, 0)
            pl.semaphore_wait(barrier, count)
            for e in range(1, ntp):
                greet(ready, "tp", e)

        @pl.when(core != 0)
        def _():
            pl.semaphore_wait(ready, 1)

    small = (draise_hbm, dbias_hbm, rraise_hbm, rbias_hbm, tempo_hbm, extra_hbm, gain_hbm)
    sources = (x_hbm, in_gain_hbm, dl_hbm, rl_hbm, wk_hbm, wr_hbm, wv_hbm, wi_hbm)
    sources += small + (mix_hbm, wa_hbm, wp_hbm)
    small = (draise_ref, dbias_ref, rraise_ref, rbias_ref, tempo_ref, extra_ref, gain_ref)
    targets = (x_ref, in_gain_ref, dl_ref, rl_ref, wk_ref, wr_ref, wv_ref, wi_ref)
    targets += small + (mix_ref, wa_ref, wp_ref)
    loads = [
        pltpu.make_async_copy(source, target, loaded.at[i])
        for i, (source, target) in enumerate(zip(sources, targets))
    ]
    for load in loads:
        load.start()
    plan = group_plan(transfer_ref.shape[1])
    groups = len(plan)

    STATE, NEAR, MAP, SKIP = range(4)
    places = (z, nsp - 1 - z)
    odd = [lax.rem(place, 2) == 1 for place in places]

    def both(*tests):
        result = tests[0]
        for test in tests[1:]:
            result = jnp.logical_and(result, test)
        return result

    def state_copy(kind, d, g):
        span = pl.ds(plan[g][0], plan[g][1])
        source = (onto_next, leaving, transfer_ref, onto_next)[kind]
        target = (incoming, near_state, near_map, skipped)[kind]
        step = (after, prev) if kind != SKIP else (after2, prev2)
        return remote(
            source.at[d, span],
            target.at[d, span],
            ss.at[kind, d, g],
            sr.at[kind, d, g],
            "sp",
            step[d],
        )

    def starts(d):
        place = places[d]
        goes = place < nsp - 1
        return (
            (STATE, both(odd[d], goes)),
            (NEAR, both(jnp.logical_not(odd[d]), goes)),
            (MAP, both(jnp.logical_not(odd[d]), goes, place > 0)),
            (SKIP, both(odd[d], place < nsp - 2)),
        )

    halo_copies = [
        remote(edge.at[1], halo.at[0], hs.at[0], hr.at[0], "sp", after),
        remote(edge.at[0], halo.at[1], hs.at[1], hr.at[1], "sp", prev),
    ]
    sends = [has_next, has_prev]
    takes = [has_prev, has_next]

    def pairs_of(g):
        return range(plan[g][0], plan[g][0] + plan[g][1])

    def mix_step(g, *operands):
        mix_group(plan[g][0], *operands)
        for d in range(2):

            @pl.when(places[d] == 0)
            def _():
                for p in pairs_of(g):
                    incoming[d, p] = jnp.zeros_like(incoming[d, p])

            for p in pairs_of(g):
                leaving[d, p] = carried_ref[d, p].astype(bf16)
            for kind, goes in starts(d)[NEAR : MAP + 1]:
                pl.when(goes)(lambda: state_copy(kind, d, g).start())

    def doubled(state):
        top0 = lax.broadcasted_iota(jnp.int32, state.shape, 1) < HEAD
        state = state.astype(f32)
        return jnp.concatenate([jnp.where(top0, state, 0.0), jnp.where(top0, 0.0, state)], 0)

    def moved(by, state):
        both_halves = dot(by, doubled(state))
        return both_halves[:HEAD] + both_halves[HEAD:]

    def relay(d, g):
        place = places[d]

        @pl.when(odd[d])
        def _():
            state_copy(NEAR, d, g).wait_recv()

            @pl.when(place == 1)
            def _():
                for p in pairs_of(g):
                    incoming[d, p] = near_state[d, p]

            @pl.when(place > 1)
            def _():
                state_copy(MAP, d, g).wait_recv()
                state_copy(SKIP, d, g).wait_recv()
                for p in pairs_of(g):
                    incoming[d, p] = (
                        moved(near_map[d, p], skipped[d, p]) + near_state[d, p].astype(f32)
                    ).astype(bf16)

            @pl.when(place < nsp - 1)
            def _():
                for p in pairs_of(g):
                    onto_next[d, p] = (
                        moved(transfer_ref[d, p], incoming[d, p]) + carried_ref[d, p]
                    ).astype(bf16)
                state_copy(STATE, d, g).start()
                pl.when(place < nsp - 2)(lambda: state_copy(SKIP, d, g).start())

        @pl.when(both(jnp.logical_not(odd[d]), place > 0))
        def _():
            state_copy(STATE, d, g).wait_recv()

    early = 2 * z < nsp

    def relays(near, g):
        @pl.when(early)
        def _():
            relay(0 if near else 1, g)

        @pl.when(jnp.logical_not(early))
        def _():
            relay(1 if near else 0, g)

    settle_pool, finish_front = front_part(
        nfs,
        x_ref,
        in_gain_ref,
        (wk_ref, wr_ref, wv_ref, wi_ref),
        (dl_ref, rl_ref),
        loads[:15],
        pool_ref,
        lat_ref,
        mine,
        cells,
        part,
        pool_part,
        onward,
        pool_onward,
        landed,
        pool_landed,
        joined,
        pool_joined,
        xs,
        xr,
        ps,
        pr,
        qs,
        qr,
        nfs + ntp - 2,
        greet_line,
        meet_line,
        lambda g: prepare_group(
            plan[g][0],
            plan[g][1],
            lat_ref,
            draise_ref,
            dbias_ref,
            rraise_ref,
            rbias_ref,
            tempo_ref,
            extra_ref,
            fade_ref,
            grow_ref,
        ),
        lambda g, key, receptance, value: mix_step(
            g,
            key,
            receptance,
            value,
            fade_ref,
            grow_ref,
            query_ref,
            local_ref,
            transfer_ref,
            carried_ref,
        ),
    )
    for load in loads[15:]:
        load.wait()
    first, second, across = routes(me, nfs, core)

    def act_part(seq, k):
        if k == 0:
            return act.at[seq, 0]
        at, count = plan[k - 1]
        return act.at[seq, 1, :, pl.ds(at * LANES, count * LANES)]

    def share(k, seq, way, peer):
        return remote(
            act_part(seq, k), act_part(seq, k), gs.at[k, way], gr.at[k, way], "fs", peer
        )

    whole_way = groups

    def share_out(k):
        if k == whole_way:
            share(k, me, 2, across).start()
        share(k, me, 0, first).start()
        share(k, me, 1, second).start()

    def pass_on(k):
        share(k, first, 0, first).wait_recv()
        if k != whole_way:
            share(k, first, 2, second).start()

    head0 = lax.broadcasted_iota(jnp.int32, (tokens, LANES), 1) < HEAD

    def head_mean(values):
        low = jnp.sum(jnp.where(head0, values, 0.0), axis=-1, keepdims=True)
        high = jnp.sum(jnp.where(head0, 0.0, values), axis=-1, keepdims=True)
        return jnp.where(head0, low, high) * (1.0 / HEAD)

    def finish_group(g):
        with jax.named_scope(f"relayB{g}"):
            relays(False, g)
        with jax.named_scope(f"readout{g}"):
            for p in pairs_of(g):
                lanes = slice(p * LANES, (p + 1) * LANES)
                readout = local_ref[:, lanes]
                for d in range(2):
                    readout = readout + dot(query_ref[d, :, lanes], doubled(incoming[d, p]))
                centred = readout - head_mean(readout)
                scaled = centred * lax.rsqrt(head_mean(centred * centred) + head_eps)
                act[me, 1, :, lanes] = (
                    scaled * gain_ref[lanes].astype(f32).reshape(1, -1)
                ).astype(bf16)
            share_out(1 + g)

    for g in range(groups - 1):
        with jax.named_scope(f"relayA{g}"):
            relays(True, g)
    settle_pool()
    edge[0] = pool_ref[:HALO]
    edge[1] = pool_ref[tokens - HALO :]
    for d in range(2):
        pl.when(sends[d])(lambda: halo_copies[d].start())
    with jax.named_scope("relayAlast"):
        relays(True, groups - 1)
    for g in range(groups - 1):
        finish_group(g)
    with jax.named_scope("halo"):
        for d in range(2):

            @pl.when(takes[d])
            def _():
                halo_copies[d].wait_recv()

            @pl.when(jnp.logical_not(takes[d]))
            def _():
                halo[d] = jnp.zeros_like(halo[d])

    span = tokens + 2 * HALO
    rim = jnp.concatenate([halo[0], pool_ref[...], halo[1]], 0)
    here = lax.broadcasted_iota(jnp.int32, (tokens, span), 0)
    there = lax.broadcasted_iota(jnp.int32, (tokens, span), 1) - HALO
    position = z * tokens + lax.broadcasted_iota(jnp.int32, (tokens, GROUP_WIDTH), 0)
    length = tokens * nsp
    groups_here = channels // GROUP_WIDTH
    for member in range(groups_here):
        cols = slice(member * GROUP_WIDTH, (member + 1) * GROUP_WIDTH)
        reach = jnp.left_shift(1, core * groups_here + member)
        window = jnp.where((there >= here - reach) & (there < here + reach), 1.0, 0.0)
        total = dot(window, rim[:, cols])
        size = (
            jnp.minimum(position + reach, length) - jnp.maximum(position - reach, 0)
        ).astype(f32)
        diff = (total / size - pool_ref[:, cols].astype(f32)).astype(bf16)
        act[me, 0, :, cols] = dot(diff, mix_ref[member]).astype(bf16)
    share_out(0)

    finish_group(groups - 1)

    other = lax.rem(core + 1, ntp)
    mine_at = pl.multiple_of(core * half_rows, half_rows)
    other_at = pl.multiple_of(other * half_rows, half_rows)

    def product(seq, k):
        if k == 0:
            return dot_rows(act[seq, 0], wp_ref[...])
        at, count = plan[k - 1]
        cols = slice(at * LANES, (at + count) * LANES)
        return dot_rows(act[seq, 1, :, cols], wa_ref[:, cols])

    def swap_of(i):
        return remote(tsend.at[i], trecv.at[i], ts.at[i], tr.at[i], "tp", other)

    def offer(i, total):
        sums_ref[i] = total
        tsend[i] = sums_ref[i, pl.ds(other_at, half_rows)].astype(bf16)
        swap_of(i).start()

    place = out_hbm.at[0, :, pl.ds(pl.multiple_of(me * depth, depth), depth)]

    def back(i, seq):
        return remote(osend.at[i], place, os.at[i], orr.at[i], "fs", seq)

    own_out = pltpu.make_async_copy(osend.at[0], place, os.at[0])

    def settle_out(i, seq):
        swap_of(i).wait_recv()
        osend[i] = (
            sums_ref[i, pl.ds(mine_at, half_rows)] + trecv[i].astype(f32)
        ).astype(bf16)
        (back(i, seq) if i else own_out).start()

    with jax.named_scope("prodown"):
        offer(0, sum(product(me, k) for k in range(1 + groups)))
    peers = ((1, flipped(me, 1)), (2, flipped(me, nfs // 2)), (3, across))
    turn = list(range(1, groups)) + [0]
    for k in turn:
        with jax.named_scope(f"pass{k}"):
            pass_on(k)
            share(k, second, 1, second).wait_recv()
        with jax.named_scope(f"prod{k}"):
            for i, seq in peers[:2]:
                sums_ref[i] = product(seq, k) + (sums_ref[i] if k != turn[0] else 0.0)
        if k == turn[0]:
            settle_out(0, me)
    k = groups
    with jax.named_scope(f"wait{k}1"):
        share(k, first, 0, first).wait_recv()
        share(k, second, 1, second).wait_recv()
    for i, seq in peers[:2]:
        with jax.named_scope(f"prod{k}{i}"):
            offer(i, product(seq, k) + sums_ref[i])
    for k in turn + [groups]:
        with jax.named_scope(f"wait{k}3"):
            share(k, across, 2, across).wait_recv()
        with jax.named_scope(f"prod{k}3"):
            total = product(across, k) + (sums_ref[3] if k != turn[0] else 0.0)
            if k < groups:
                sums_ref[3] = total
            else:
                offer(3, total)
        if k == turn[0]:
            for i, seq in peers[:2]:
                with jax.named_scope(f"swapwait{i}"):
                    settle_out(i, seq)
    with jax.named_scope("swapwait3"):
        settle_out(3, across)
    with jax.named_scope("retwait"):
        for i, seq in peers:
            back(i, seq).wait_recv()
    own_out.wait()
    for k in range(1 + groups):
        for way in range(3):
            share(k, me, way, first).wait_send()
    for i in range(1 + len(peers)):
        swap_of(i).wait_send()
    for i, seq in peers:
        back(i, seq).wait_send()
    for d in range(2):

        @pl.when(sends[d])
        def _():
            halo_copies[d].wait_send()

        for kind, goes in starts(d):

            @pl.when(goes)
            def _():
                for g in range(groups):
                    state_copy(kind, d, g).wait_send()
    finish_front()


def shards(
    inputs,
    input_norm_gain,
    receptance_matrix,
    key_matrix,
    value_matrix,
    pooling_input_weight,
    decay_lower_matrix,
    decay_raise_matrix,
    decay_offset_bias,
    removal_lower_matrix,
    removal_raise_matrix,
    removal_rate_bias,
    tempo_scale,
    sudden_decay_extra,
    head_norm_gain,
    group_mixing_weight,
    attention_output_matrix,
    pooling_output_matrix,
):
    nsp, nfs, ntp = lax.axis_size("sp"), lax.axis_size("fs"), lax.axis_size("tp")
    _, tokens, features = inputs.shape
    depth, channels = key_matrix.shape
    pairs = channels // LANES
    groups = len(group_plan(pairs))
    dma = pltpu.SemaphoreType.DMA
    rank = decay_lower_matrix.shape[1]
    rank2 = decay_raise_matrix.shape[0] * decay_raise_matrix.shape[1]
    anywhere = pl.BlockSpec(memory_space=pl.ANY)
    half = (nfs, tokens // ntp, depth)
    return pl.pallas_call(
        functools.partial(layer_kernel, nsp, nfs, ntp),
        out_shape=pltpu.VMEM((1, tokens // ntp, features), bf16),
        in_specs=[anywhere] * 18,
        out_specs=anywhere,
        scratch_shapes=[
            pltpu.VMEM(inputs.shape, bf16),
            pltpu.VMEM(input_norm_gain.shape, bf16),
            pltpu.VMEM((rank2, channels), bf16),
            pltpu.VMEM(decay_offset_bias.shape, f32),
            pltpu.VMEM((rank2, channels), bf16),
            pltpu.VMEM(removal_rate_bias.shape, f32),
            pltpu.VMEM(tempo_scale.shape[1:], f32),
            pltpu.VMEM(sudden_decay_extra.shape[1:], f32),
            pltpu.VMEM(head_norm_gain.shape, bf16),
        ]
        + [pltpu.VMEM((depth, channels), bf16)] * 4
        + [
            pltpu.VMEM((features, rank), bf16),
            pltpu.VMEM((features, rank), bf16),
            pltpu.VMEM(group_mixing_weight.shape, bf16),
            pltpu.VMEM(attention_output_matrix.shape, bf16),
            pltpu.VMEM(pooling_output_matrix.shape, bf16),
            dma((18,)),
            pltpu.VMEM((nfs, tokens, depth), bf16),
            pltpu.VMEM((nfs, tokens, depth), bf16),
            pltpu.VMEM((2, pairs, 3, tokens, LANES), bf16),
            pltpu.VMEM((2, tokens, channels), bf16),
            pltpu.VMEM((pairs, 3, tokens, LANES), bf16),
            pltpu.VMEM((tokens, channels), bf16),
            pltpu.VMEM((2, pairs, 3, tokens, LANES), bf16),
            pltpu.VMEM((2, tokens, channels), bf16),
            pltpu.VMEM((pairs, 3, tokens, LANES), bf16),
            pltpu.VMEM((tokens, channels), bf16),
            dma((nfs, ntp)),
            dma((nfs, 2)),
            pltpu.SemaphoreType.REGULAR,
            dma((groups + 1, 2)),
            dma((groups + 1, 2)),
            dma((groups + 1,)),
            dma((groups + 1,)),
            pltpu.VMEM((2, tokens, rank), bf16),
            pltpu.VMEM((2, 5, tokens, channels), f32),
            pltpu.VMEM((2, tokens // BLOCK, tokens, channels), f32),
            pltpu.VMEM((tokens, channels), bf16),
            pltpu.VMEM((2, tokens, channels), bf16),
            pltpu.VMEM((tokens, channels), f32),
            pltpu.VMEM((2, pairs, LANES, LANES), bf16),
            pltpu.VMEM((2, pairs, HEAD, LANES), f32),
            pltpu.VMEM((2, HALO, channels), bf16),
            pltpu.VMEM((2, HALO, channels), bf16),
            pltpu.VMEM((2, pairs, HEAD, LANES), bf16),
            pltpu.VMEM((2, pairs, HEAD, LANES), bf16),
            pltpu.VMEM((2, pairs, HEAD, LANES), bf16),
            pltpu.VMEM((2, pairs, LANES, LANES), bf16),
            pltpu.VMEM((2, pairs, HEAD, LANES), bf16),
            pltpu.VMEM((2, pairs, HEAD, LANES), bf16),
            pltpu.VMEM((nfs, 2, tokens, channels), bf16),
            pltpu.VMEM(half, bf16),
            pltpu.VMEM(half, bf16),
            pltpu.VMEM((nfs, tokens, depth), f32),
            pltpu.VMEM(half, bf16),
            dma((2,)),
            dma((2,)),
            dma((4, 2, groups)),
            dma((4, 2, groups)),
            dma((1 + groups, 3)),
            dma((1 + groups, 3)),
            dma((nfs,)),
            dma((nfs,)),
            dma((nfs,)),
            dma((nfs,)),
        ],
        compiler_params=pltpu.CompilerParams(
            collective_id=0, has_side_effects=True, vmem_limit_bytes=60 * 1024 * 1024
        ),
        name="layer",
    )(
        inputs,
        input_norm_gain,
        key_matrix,
        receptance_matrix,
        value_matrix,
        pooling_input_weight,
        decay_lower_matrix,
        removal_lower_matrix,
        decay_raise_matrix.reshape(rank2, channels),
        decay_offset_bias,
        removal_raise_matrix.reshape(rank2, channels),
        removal_rate_bias,
        tempo_scale[0],
        sudden_decay_extra[0],
        group_mixing_weight,
        head_norm_gain,
        attention_output_matrix,
        pooling_output_matrix,
    )


def solution(mesh):
    in_specs = (
        P("fs", "sp", None),
        P(),
        P("fs", "tp"),
        P("fs", "tp"),
        P("fs", "tp"),
        P("fs", "tp"),
        P(),
        P(None, None, "tp"),
        P(None, "tp"),
        P(),
        P(None, None, "tp"),
        P(None, "tp"),
        P("fs", None, "tp", "sp"),
        P("fs", None, "tp", "sp"),
        P("tp"),
        P("tp", None, None),
        P("fs", "tp"),
        P("fs", "tp"),
    )
    out_specs = P("fs", ("sp", "tp"), None)
    return jax.shard_map(shards, mesh=mesh, in_specs=in_specs, out_specs=out_specs, check_vma=False)
```

time: 58.4 us -> 52.3 us (0.90)
  Pallas kernels: 56.6 us -> 51.5 us
  local copies, waits for them, and re-layouts: 1.67 us -> 0.71 us
    pallas_call x1, Pallas kernels: 56.6 us -> 51.5 us  [shards(): pl.pallas_call(functools.partial(layer_kernel, nsp, nfs, ntp), out_shape=...]
    unnamed x1, local copies, waits for them, and re-layouts: 1.67 us -> 0.71 us
where the time goes in v2:
time: 52.3 us; the launch traced here: 52.2 us
  Pallas kernels  51.5 us (98%)
  local copies, waits for them, and re-layouts  0.71 us (1%)
    pallas_call x1, Pallas kernels, shards(): pl.pallas_call(functools.partial(layer_kernel, nsp, nfs, ntp), out_shape=...  51.5 us

profile of v2, /device:TPU:0, one launch (start us, length us, event | category | flops | bytes accessed | tf_op | source)
XLA Modules:
  0.0 52.2 jit_solution(17263573974186706353)
XLA Ops:
  0.0 51.5 %layer.1 = bf16[1,64,2048]{2,1,0:T(8,128)(2,1)S(1)} custom-call(bf16[1,128,2048]{2,1,0:T(8,128)(2,1)} %x_hbm.1, bf16[2048]{0:T(1024)(128)(2,1)} %in_gain_hbm.1, bf16[512,512]{1,0:T(8,128)(2,1)} %wk_hbm.1, bf16[512,512]{1,0:T(8,128)(2,1)} %wr_hbm.1, bf16[512,512]{1,0:T(8,128)(2,1)} %wv_hbm.1, bf16[512,512]{1,0:T(8,128)(2,1)} %wi_hbm.1, ...), custom_call_target="tpu_custom_call" | custom-call | tf_op jit(solution)/shard_map/layer/pallas_call | solution.py:1111
  51.5 0.7 %copy.20 = bf16[1,64,2048]{2,1,0:T(8,128)(2,1)} copy(bf16[1,64,2048]{2,1,0:T(8,128)(2,1)S(1)} %layer.1) | data formatting | bytes 524288

commit v3 on v2

--- a/solution.py
+++ b/solution.py
@@ -88,6 +88,7 @@
     cells,
     part,
     pool_part,
+    own_part,
     onward,
     pool_onward,
     landed,
@@ -96,13 +97,14 @@
     pool_joined,
     xs,
     xr,
-    ps,
+    loaded,
     pr,
-    qs,
     qr,
     count,
     greet_line,
     meet_line,
+    send_rims,
+    own_rims,
     prepare,
     mix_group,
 ):
@@ -128,11 +130,11 @@
 
     def row_copy(d):
         peer = flipped(me, d)
-        return remote(mine.at[peer], cells.at[me], xs.at[d, 0], xr.at[d, 0], "fs", peer)
+        return remote(mine.at[peer], cells.at[me], xs.at[d - 1, 0], xr.at[d - 1], "fs", peer)
 
     def pass_copy(d, e):
         at = cells.at[flipped(me, d)]
-        return remote(at, at, xs.at[d, 1 + e], xr.at[d, 1], "tp", e)
+        return remote(at, at, xs.at[d - 1, 1 + e], xr.at[d - 1], "tp", e)
 
     with jax.named_scope("barrier"):
 
@@ -182,7 +184,7 @@
         return remote(
             part.at[slot, span_of(g)],
             landed.at[slot, span_of(g)],
-            ps.at[g, slot],
+            loaded.at[2 * g + slot],
             pr.at[g, slot],
             "fs",
             first,
@@ -192,7 +194,7 @@
         return remote(
             pool_part.at[slot],
             pool_landed.at[slot],
-            ps.at[groups, slot],
+            loaded.at[2 * groups + slot],
             pr.at[groups, slot],
             "fs",
             first,
@@ -200,11 +202,11 @@
 
     def second_copy(g):
         return remote(
-            onward.at[span_of(g)], joined.at[span_of(g)], qs.at[g], qr.at[g], "fs", second
+            onward.at[span_of(g)], joined.at[span_of(g)], loaded.at[2 * groups + 2 + g], qr.at[g], "fs", second
         )
 
     second_pool = remote(
-        pool_onward, pool_joined, qs.at[groups], qr.at[groups], "fs", second
+        pool_onward, pool_joined, loaded.at[3 * groups + 2], qr.at[groups], "fs", second
     )
 
     def piece(m, g):
@@ -229,30 +231,40 @@
 
     def forward(g):
         with jax.named_scope(f"fwd{g}"):
+            terms = [dot(cells[second], piece(m, g)) for m in range(3)]
             first_copy(g, 1).wait_recv()
             for m in range(3):
-                keep(
-                    onward, g, m, dot(cells[second], piece(m, g)) + beside(landed.at[1], g, m)
-                )
+                keep(onward, g, m, terms[m] + beside(landed.at[1], g, m))
             second_copy(g).start()
+
+    def ready_pool():
+        with jax.named_scope("readypool"):
+            for slot in (1, 0):
+                pool_part[slot] = dot(cells[targets[slot]], weights[3][...]).astype(bf16)
+            own_rims(lambda rows: dot(mine[me, rows], weights[3][...]))
 
     def begin_pool():
         with jax.named_scope("beginpool"):
+            send_rims(1, pool_part.at[0], first)
             for slot in (1, 0):
-                pool_part[slot] = dot(cells[targets[slot]], weights[3][...]).astype(bf16)
                 first_pool(slot).start()
 
     def forward_pool():
         with jax.named_scope("fwdpool"):
+            term = dot(cells[second], weights[3][...])
             first_pool(1).wait_recv()
-            pool_onward[...] = (
-                dot(cells[second], weights[3][...]) + pool_landed[1].astype(f32)
-            ).astype(bf16)
+            pool_onward[...] = (term + pool_landed[1].astype(f32)).astype(bf16)
+            send_rims(2, pool_onward, second)
             second_pool.start()
 
     def prep(g):
         with jax.named_scope(f"prep{g}"):
             prepare(g)
+            at, count = plan[g]
+            for m in range(3):
+                term = dot(mine[me], piece(m, g))
+                for j in range(count):
+                    own_part[at + j, m] = term[:, j * LANES : (j + 1) * LANES]
 
     def settle(g):
         with jax.named_scope(f"settle{g}"):
@@ -261,7 +273,7 @@
         with jax.named_scope(f"mix{g}"):
             owned = [
                 (
-                    dot(mine[me], piece(m, g))
+                    beside(own_part, g, m)
                     + beside(landed.at[0], g, m)
                     + beside(joined, g, m)
                 ).astype(bf16)
@@ -272,10 +284,11 @@
     prep(0)
     forward(0)
     prep(1)
+    prep(2)
     forward(1)
-    prep(2)
     meet_line()
     settle(0)
+    ready_pool()
     forward(2)
     begin_pool()
     settle(1)
@@ -283,10 +296,11 @@
     settle(2)
     def settle_pool():
         with jax.named_scope("poolin"):
+            term = dot(mine[me], weights[3][...])
             first_pool(0).wait_recv()
             second_pool.wait_recv()
             pool_ref[...] = (
-                dot(mine[me], weights[3][...])
+                term
                 + pool_landed[0].astype(f32)
                 + pool_joined[...].astype(f32)
             ).astype(bf16)
@@ -299,6 +313,7 @@
                 for e in range(ntp - 1):
                     pass_copy(d, e).wait_send()
 
+    def free_sends():
         for g in range(groups):
             for slot in (1, 0):
                 first_copy(g, slot).wait_send()
@@ -307,7 +322,7 @@
             first_pool(slot).wait_send()
         second_pool.wait_send()
 
-    return settle_pool, finish
+    return free_sends, settle_pool, finish
 
 
 def group_plan(pairs):
@@ -616,6 +631,7 @@
     cells,
     part,
     pool_part,
+    own_part,
     onward,
     pool_onward,
     landed,
@@ -625,9 +641,7 @@
     xs,
     xr,
     ready,
-    ps,
     pr,
-    qs,
     qr,
     lat_ref,
     fade_ref,
@@ -639,6 +653,7 @@
     carried_ref,
     edge,
     halo,
+    rims,
     incoming,
     leaving,
     near_state,
@@ -654,7 +669,6 @@
     hr,
     ss,
     sr,
-    gs,
     gr,
     ts,
     tr,
@@ -741,8 +755,8 @@
         return remote(
             source.at[d, span],
             target.at[d, span],
-            ss.at[kind, d, g],
-            sr.at[kind, d, g],
+            ss.at[(0, 0, 1, 1)[kind], d, g],
+            sr.at[(0, 0, 1, 2)[kind], d, g],
             "sp",
             step[d],
         )
@@ -757,10 +771,27 @@
             (SKIP, both(odd[d], place < nsp - 2)),
         )
 
-    halo_copies = [
-        remote(edge.at[1], halo.at[0], hs.at[0], hr.at[0], "sp", after),
-        remote(edge.at[0], halo.at[1], hs.at[1], hr.at[1], "sp", prev),
-    ]
+    ends = (pl.ds(tokens - HALO, HALO), pl.ds(0, HALO))
+
+    def rim_copy(c, d, source, owner):
+        return pltpu.make_async_remote_copy(
+            src_ref=source,
+            dst_ref=rims.at[d, c],
+            send_sem=hs.at[c, d],
+            recv_sem=hr.at[c, d],
+            device_id={"fs": owner, "sp": after if d == 0 else prev},
+            device_id_type=pl.DeviceIdType.MESH,
+        )
+
+    def send_rims(c, source, owner):
+        for d in range(2):
+            pl.when(sends[d])(lambda: rim_copy(c, d, source.at[ends[d]], owner).start())
+
+    def own_rims(rows_of):
+        for d in range(2):
+            edge[d] = rows_of(ends[d]).astype(bf16)
+            pl.when(sends[d])(lambda: rim_copy(0, d, edge.at[d], me).start())
+
     sends = [has_next, has_prev]
     takes = [has_prev, has_next]
 
@@ -835,7 +866,7 @@
         def _():
             relay(1 if near else 0, g)
 
-    settle_pool, finish_front = front_part(
+    free_sends, settle_pool, finish_front = front_part(
         nfs,
         x_ref,
         in_gain_ref,
@@ -848,6 +879,7 @@
         cells,
         part,
         pool_part,
+        own_part,
         onward,
         pool_onward,
         landed,
@@ -856,13 +888,14 @@
         pool_joined,
         xs,
         xr,
-        ps,
+        loaded,
         pr,
-        qs,
         qr,
         nfs + ntp - 2,
         greet_line,
         meet_line,
+        send_rims,
+        own_rims,
         lambda g: prepare_group(
             plan[g][0],
             plan[g][1],
@@ -901,7 +934,7 @@
 
     def share(k, seq, way, peer):
         return remote(
-            act_part(seq, k), act_part(seq, k), gs.at[k, way], gr.at[k, way], "fs", peer
+            act_part(seq, k), act_part(seq, k), loaded.at[3 * k + way], gr.at[k, way], "fs", peer
         )
 
     whole_way = groups
@@ -943,21 +976,16 @@
     for g in range(groups - 1):
         with jax.named_scope(f"relayA{g}"):
             relays(True, g)
+    free_sends()
     settle_pool()
-    edge[0] = pool_ref[:HALO]
-    edge[1] = pool_ref[tokens - HALO :]
-    for d in range(2):
-        pl.when(sends[d])(lambda: halo_copies[d].start())
-    with jax.named_scope("relayAlast"):
-        relays(True, groups - 1)
-    for g in range(groups - 1):
-        finish_group(g)
     with jax.named_scope("halo"):
         for d in range(2):
 
             @pl.when(takes[d])
             def _():
-                halo_copies[d].wait_recv()
+                for c in range(3):
+                    rim_copy(c, d, edge.at[d], me).wait_recv()
+                halo[d] = sum(rims[d, c].astype(f32) for c in range(3)).astype(bf16)
 
             @pl.when(jnp.logical_not(takes[d]))
             def _():
@@ -982,6 +1010,10 @@
         act[me, 0, :, cols] = dot(diff, mix_ref[member]).astype(bf16)
     share_out(0)
 
+    with jax.named_scope("relayAlast"):
+        relays(True, groups - 1)
+    for g in range(groups - 1):
+        finish_group(g)
     finish_group(groups - 1)
 
     other = lax.rem(core + 1, ntp)
@@ -1020,7 +1052,7 @@
     with jax.named_scope("prodown"):
         offer(0, sum(product(me, k) for k in range(1 + groups)))
     peers = ((1, flipped(me, 1)), (2, flipped(me, nfs // 2)), (3, across))
-    turn = list(range(1, groups)) + [0]
+    turn = list(range(groups))
     for k in turn:
         with jax.named_scope(f"pass{k}"):
             pass_on(k)
@@ -1052,30 +1084,32 @@
                     settle_out(i, seq)
     with jax.named_scope("swapwait3"):
         settle_out(3, across)
+    with jax.named_scope("sent"):
+        own_out.wait()
+        for k in range(1 + groups):
+            for way in range(3):
+                share(k, me, way, first).wait_send()
+        for i in range(1 + len(peers)):
+            swap_of(i).wait_send()
+        for i, seq in peers:
+            back(i, seq).wait_send()
+        for d in range(2):
+
+            @pl.when(sends[d])
+            def _():
+                for c in range(3):
+                    rim_copy(c, d, edge.at[d], me).wait_send()
+
+            for kind, goes in starts(d):
+
+                @pl.when(goes)
+                def _():
+                    for g in range(groups):
+                        state_copy(kind, d, g).wait_send()
+        finish_front()
     with jax.named_scope("retwait"):
         for i, seq in peers:
             back(i, seq).wait_recv()
-    own_out.wait()
-    for k in range(1 + groups):
-        for way in range(3):
-            share(k, me, way, first).wait_send()
-    for i in range(1 + len(peers)):
-        swap_of(i).wait_send()
-    for i, seq in peers:
-        back(i, seq).wait_send()
-    for d in range(2):
-
-        @pl.when(sends[d])
-        def _():
-            halo_copies[d].wait_send()
-
-        for kind, goes in starts(d):
-
-            @pl.when(goes)
-            def _():
-                for g in range(groups):
-                    state_copy(kind, d, g).wait_send()
-    finish_front()
 
 
 def shards(
@@ -1136,18 +1170,17 @@
             pltpu.VMEM((nfs, tokens, depth), bf16),
             pltpu.VMEM((2, pairs, 3, tokens, LANES), bf16),
             pltpu.VMEM((2, tokens, channels), bf16),
+            pltpu.VMEM((pairs, 3, tokens, LANES), f32),
             pltpu.VMEM((pairs, 3, tokens, LANES), bf16),
             pltpu.VMEM((tokens, channels), bf16),
             pltpu.VMEM((2, pairs, 3, tokens, LANES), bf16),
             pltpu.VMEM((2, tokens, channels), bf16),
             pltpu.VMEM((pairs, 3, tokens, LANES), bf16),
             pltpu.VMEM((tokens, channels), bf16),
-            dma((nfs, ntp)),
-            dma((nfs, 2)),
+            dma((nfs - 1, ntp)),
+            dma((nfs - 1,)),
             pltpu.SemaphoreType.REGULAR,
             dma((groups + 1, 2)),
-            dma((groups + 1, 2)),
-            dma((groups + 1,)),
             dma((groups + 1,)),
             pltpu.VMEM((2, tokens, rank), bf16),
             pltpu.VMEM((2, 5, tokens, channels), f32),
@@ -1159,6 +1192,7 @@
             pltpu.VMEM((2, pairs, HEAD, LANES), f32),
             pltpu.VMEM((2, HALO, channels), bf16),
             pltpu.VMEM((2, HALO, channels), bf16),
+            pltpu.VMEM((2, 3, HALO, channels), bf16),
             pltpu.VMEM((2, pairs, HEAD, LANES), bf16),
             pltpu.VMEM((2, pairs, HEAD, LANES), bf16),
             pltpu.VMEM((2, pairs, HEAD, LANES), bf16),
@@ -1170,11 +1204,10 @@
             pltpu.VMEM(half, bf16),
             pltpu.VMEM((nfs, tokens, depth), f32),
             pltpu.VMEM(half, bf16),
-            dma((2,)),
-            dma((2,)),
-            dma((4, 2, groups)),
-            dma((4, 2, groups)),
-            dma((1 + groups, 3)),
+            dma((3, 2)),
+            dma((3, 2)),
+            dma((2, 2, groups)),
+            dma((3, 2, groups)),
             dma((1 + groups, 3)),
             dma((nfs,)),
             dma((nfs,)),

time: 52.3 us -> 50.2 us (0.960)
  Pallas kernels: 51.5 us -> 49.3 us
    pallas_call x1, Pallas kernels: 51.5 us -> 49.3 us  [shards(): pl.pallas_call(functools.partial(layer_kernel, nsp, nfs, ntp), out_shape=...]
where the time goes in v3:
time: 50.2 us; the launch traced here: 50 us
  Pallas kernels  49.3 us (98%)
  local copies, waits for them, and re-layouts  0.71 us (1%)
    pallas_call x1, Pallas kernels, shards(): pl.pallas_call(functools.partial(layer_kernel, nsp, nfs, ntp), out_shape=...  49.3 us

profile of v3, /device:TPU:0, one launch (start us, length us, event | category | flops | bytes accessed | tf_op | source)
XLA Modules:
  0.0 50.0 jit_solution(7624016483601809427)
XLA Ops:
  0.0 49.3 %layer.1 = bf16[1,64,2048]{2,1,0:T(8,128)(2,1)S(1)} custom-call(bf16[1,128,2048]{2,1,0:T(8,128)(2,1)} %x_hbm.1, bf16[2048]{0:T(1024)(128)(2,1)} %in_gain_hbm.1, bf16[512,512]{1,0:T(8,128)(2,1)} %wk_hbm.1, bf16[512,512]{1,0:T(8,128)(2,1)} %wr_hbm.1, bf16[512,512]{1,0:T(8,128)(2,1)} %wv_hbm.1, bf16[512,512]{1,0:T(8,128)(2,1)} %wi_hbm.1, ...), custom_call_target="tpu_custom_call" | custom-call | tf_op jit(solution)/shard_map/layer/pallas_call | solution.py:1145
  49.3 0.7 %copy.20 = bf16[1,64,2048]{2,1,0:T(8,128)(2,1)} copy(bf16[1,64,2048]{2,1,0:T(8,128)(2,1)S(1)} %layer.1) | data formatting | bytes 524288

commit v4 on v3

--- a/solution.py
+++ b/solution.py
@@ -105,6 +105,7 @@
     meet_line,
     send_rims,
     own_rims,
+    first_relay,
     prepare,
     mix_group,
 ):
@@ -166,12 +167,12 @@
                 for e in range(ntp - 1):
                     pass_copy(d, e).start()
 
-        @pl.when(jnp.logical_not(lead))
-        def _():
-            for d in order:
+    def meet_rows(d):
+        with jax.named_scope("rows"):
+
+            @pl.when(jnp.logical_not(lead))
+            def _():
                 pass_copy(d, 0).wait_recv()
-
-        greet_line()
 
     first, second, across = routes(me, n, core)
     targets = (first, across)
@@ -225,8 +226,12 @@
     with jax.named_scope("partials"):
         for g in range(groups):
             for slot in (1, 0):
+                if g == 0 and slot:
+                    meet_rows(n // 2 + 1)
                 for m in range(3):
                     keep(part.at[slot], g, m, dot(cells[targets[slot]], piece(m, g)))
+                if g == 0 and slot:
+                    meet_rows(1)
                 first_copy(g, slot).start()
 
     def forward(g):
@@ -281,6 +286,8 @@
             ]
             mix_group(g, *owned)
 
+    meet_rows(n // 2)
+    greet_line()
     prep(0)
     forward(0)
     prep(1)
@@ -292,6 +299,7 @@
     forward(2)
     begin_pool()
     settle(1)
+    first_relay()
     forward_pool()
     settle(2)
     def settle_pool():
@@ -896,6 +904,7 @@
         meet_line,
         send_rims,
         own_rims,
+        lambda: relays(True, 0),
         lambda g: prepare_group(
             plan[g][0],
             plan[g][1],
@@ -973,9 +982,10 @@
                 ).astype(bf16)
             share_out(1 + g)
 
-    for g in range(groups - 1):
+    for g in range(1, groups - 1):
         with jax.named_scope(f"relayA{g}"):
             relays(True, g)
+    finish_group(0)
     free_sends()
     settle_pool()
     with jax.named_scope("halo"):
@@ -1012,7 +1022,7 @@
 
     with jax.named_scope("relayAlast"):
         relays(True, groups - 1)
-    for g in range(groups - 1):
+    for g in range(1, groups - 1):
         finish_group(g)
     finish_group(groups - 1)
 

time: 50.2 us -> 49.9 us (level)
  no operation moved by 1% of the time
where the time goes in v4:
time: 49.9 us; the launch traced here: 49.7 us
  Pallas kernels  49 us (98%)
  local copies, waits for them, and re-layouts  0.71 us (1%)
    pallas_call x1, Pallas kernels, shards(): pl.pallas_call(functools.partial(layer_kernel, nsp, nfs, ntp), out_shape=...  49 us

profile of v4, /device:TPU:0, one launch (start us, length us, event | category | flops | bytes accessed | tf_op | source)
XLA Modules:
  0.0 49.7 jit_solution(12293136705718998141)
XLA Ops:
  0.0 49.0 %layer.1 = bf16[1,64,2048]{2,1,0:T(8,128)(2,1)S(1)} custom-call(bf16[1,128,2048]{2,1,0:T(8,128)(2,1)} %x_hbm.1, bf16[2048]{0:T(1024)(128)(2,1)} %in_gain_hbm.1, bf16[512,512]{1,0:T(8,128)(2,1)} %wk_hbm.1, bf16[512,512]{1,0:T(8,128)(2,1)} %wr_hbm.1, bf16[512,512]{1,0:T(8,128)(2,1)} %wv_hbm.1, bf16[512,512]{1,0:T(8,128)(2,1)} %wi_hbm.1, ...), custom_call_target="tpu_custom_call" | custom-call | tf_op jit(solution)/shard_map/layer/pallas_call | solution.py:1155
  49.0 0.7 %copy.20 = bf16[1,64,2048]{2,1,0:T(8,128)(2,1)} copy(bf16[1,64,2048]{2,1,0:T(8,128)(2,1)S(1)} %layer.1) | data formatting | bytes 524288
